TPU v7x, 32 devices: a whole 2x2x4 slice. The times are simulated.
32 devices in a mesh: grp: 2 (over x), ep: 16 (over z, y, core).
Axes of the slice: x: 2, y: 2, z: 4, core: 2. Of those that a mesh axis runs over, the one named last changes fastest.
Arguments:
- hidden: bfloat16 [4096, 2048], P(('grp', 'ep')), parts along dimension 0, may hold values from -6 to 6
- state: float32 [2, 4096, 4096], P(None, ('grp', 'ep')), parts along dimension 1, may hold values from -6 to 6
- norm_gain: float32 [2048], replicated, may hold values from 0.1 to 1.9
- w_in: bfloat16 [2048, 1024], P(None, 'ep'), may hold values from -0.125 to 0.125
- lam_re: float32 [64, 64], replicated, may hold values from -1 to -0.1
- lam_im: float32 [64, 64], replicated, may hold values from 0 to 200
- log_step: float32 [64], replicated, may hold values from -4.6 to -0.7
- in_re: float32 [64, 64, 16], replicated, may hold values from -1 to 1
- in_im: float32 [64, 64, 16], replicated, may hold values from -1 to 1
- out_re: float32 [64, 16, 64], replicated, may hold values from -0.75 to 0.75
- out_im: float32 [64, 16, 64], replicated, may hold values from -0.75 to 0.75
- skip: float32 [1024], replicated, may hold values from -4 to 4
- w_glu: bfloat16 [1024, 1024], replicated, may hold values from -0.1875 to 0.1875
- w_out: bfloat16 [1024, 2048], replicated, may hold values from -0.375 to 0.375
- ffn_gain: float32 [2048], replicated, may hold values from 0.1 to 1.9
- w_group: bfloat16 [2048, 4], replicated, may hold values from -0.03125 to 0.03125
- w_route: bfloat16 [2048, 16], replicated, may hold values from -0.03125 to 0.03125
- w_gate: bfloat16 [16, 2048, 512], P('ep'), may hold values from -0.125 to 0.125
- w_up: bfloat16 [16, 2048, 512], P('ep'), may hold values from -0.125 to 0.125
- w_down: bfloat16 [16, 512, 2048], P('ep'), may hold values from -2 to 2
- route_ids: int32 [4096, 2], P(('grp', 'ep')), parts along dimension 0, may hold values from 0 to 15, as said below
Outputs:
- hidden_out: bfloat16 [4096, 2048], P(('grp', 'ep')), parts along dimension 0
- new_state: float32 [2, 4096, 4096], P(None, ('grp', 'ep')), parts along dimension 1
There are 2 independent parts, one for each index of `grp`. A program takes and returns all parts, laid end to end along the dimension named above; an argument that names none is the same for every part. Nothing has to cross between parts.
Inputs may be any that keep to these rules, and one draw needn't show every extreme that they name: `route_ids`: each row names 2 different experts of one expert group (experts g * 4 to g * 4 + 3). Among the rows of one device no expert is named more than 32 times, and in every draw some experts are named exactly 32 times by the rows of every device.
All inputs are finite; a program needn't handle non-finite values.
Results may differ from a plain program's by a relative error of at most 0.013.
Values may be sent and summed in bfloat16 or wider, within the bound.
A program may use at most 128 MiB of HBM per device.

v0:
```python
import functools

import jax
import jax.numpy as jnp
from jax import lax
from jax.experimental import pallas as pl
from jax.experimental.pallas import tpu as pltpu
from jax.sharding import PartitionSpec as P

EXP_GROUPS = 4
TOPK = 2
MESH = pl.DeviceIdType.MESH
VMEM = pl.BlockSpec(memory_space=pltpu.VMEM)
ANY = pl.BlockSpec(memory_space=pl.ANY)
F32 = jnp.float32
BF16 = jnp.bfloat16
NT = (((1,), (1,)), ((), ()))
TN = (((0,), (0,)), ((), ()))
LIMIT = 60 * 1024 * 1024


def remote(src, dst, send_sem, recv_sem, device):
    return pltpu.make_async_remote_copy(
        src_ref=src, dst_ref=dst, send_sem=send_sem, recv_sem=recv_sem, device_id=device, device_id_type=MESH
    )


def greet(peers):
    barrier = pltpu.get_barrier_semaphore()
    for peer in peers:
        pl.semaphore_signal(barrier, inc=1, device_id=peer, device_id_type=MESH)
    pl.semaphore_wait(barrier, len(peers))


def gather_kernel(
    chips, hidden_ref, gain_ref, w_ref, out_ref, held, normed, zs, zr, ys, yr, xs, xr, ds, dr, es, er,
    own_s, own_r, local_sem,
):
    grp = lax.axis_index("grp")
    me = lax.axis_index("ep")
    chip, core = me // 2, me % 2
    lines = chips // 2
    line, y = chip // 2, chip % 2

    def at(row, column):
        return (grp, (row * 2 + column) * 2 + core)

    targets = [(line + i) % lines for i in range(1, lines)]
    mate = (grp, me + 1 - 2 * core)
    side = grp % 2
    across = (grp + 1 - 2 * side, me)
    beside = at(line, 1 - y)
    rows, depth = w_ref.shape
    third = depth // 3 // 128 * 128
    my_cols = pl.ds(pl.multiple_of(side * third, 128), depth - third)
    out_cols = pl.ds(pl.multiple_of(side * (depth - third), 128), third)
    in_cols = pl.ds(pl.multiple_of((1 - side) * (depth - third), 128), third)
    subs = 2
    part = rows // subs
    spans = [pl.ds(sub * part, part) for sub in range(subs)]
    sends = []

    def start(copy):
        copy.start()
        sends.append(copy)

    local = pltpu.make_async_copy(w_ref, held.at[chip, core], local_sem)
    local.start()
    greet([at(target, y) for target in targets] + [beside, mate, across])
    for i in range(lines):
        for sub in range(subs):
            src, dst = w_ref.at[spans[sub], my_cols], held.at[chip, core, spans[sub], my_cols]
            if i == 0:
                start(remote(src, dst, ys.at[0, sub], yr.at[0, sub], beside))
            else:
                start(remote(src, dst, zs.at[i, sub], zr.at[i, sub], at(targets[i - 1], y)))
    start(remote(w_ref, held.at[chip, core], own_s, own_r, mate))

    wide = hidden_ref[...].astype(F32)
    mean = jnp.mean(wide * wide, axis=-1, keepdims=True)
    normed[...] = (wide * lax.rsqrt(mean + 1e-06) * gain_ref[...]).astype(BF16)

    def origin(kind, i):
        return (line + lines - i) % lines * 2 + (y if kind == 0 else 1 - y)

    order = []
    for i in range(1, lines + 1):
        for sub in range(subs):
            if i < lines:
                order.append((0, i, sub))
            order.append((1, i - 1, sub))

    def take(kind, i, sub):
        place = origin(kind, i)
        spot = held.at[place, core, spans[sub], my_cols]
        if kind == 0:
            remote(spot, spot, zs.at[i, sub], zr.at[i, sub], mate).wait_recv()
            start(remote(spot, spot, ys.at[i, sub], yr.at[i, sub], beside))
        else:
            remote(spot, spot, ys.at[i, sub], yr.at[i, sub], mate).wait_recv()
        side_spot = held.at[place, core, spans[sub], out_cols]
        start(remote(side_spot, side_spot, xs.at[kind, i, sub], xr.at[kind, i, sub], across))
        start(remote(spot, spot, ds.at[kind, i, sub], dr.at[kind, i, sub], mate))

    def take_x(kind, i, sub):
        spot = held.at[origin(kind, i), core, spans[sub], in_cols]
        remote(spot, spot, xs.at[kind, i, sub], xr.at[kind, i, sub], mate).wait_recv()
        start(remote(spot, spot, es.at[kind, i, sub], er.at[kind, i, sub], mate))

    lag = 2 * subs
    for at_ in range(len(order) + lag):
        if at_ < len(order):
            take(*order[at_])
        if at_ >= lag:
            take_x(*order[at_ - lag])
    for kind, i, sub in order:
        place = origin(kind, i)
        spot = held.at[place, 1 - core, spans[sub], my_cols]
        remote(spot, spot, ds.at[kind, i, sub], dr.at[kind, i, sub], mate).wait_recv()
        spot = held.at[place, 1 - core, spans[sub], in_cols]
        remote(spot, spot, es.at[kind, i, sub], er.at[kind, i, sub], mate).wait_recv()
    spot = held.at[chip, 1 - core]
    remote(spot, spot, own_s, own_r, mate).wait_recv()
    local.wait()
    for pair in range(chips // 2):
        block = held[2 * pair : 2 * pair + 2].reshape(4 * rows, depth)
        product = lax.dot_general(normed[...], block, NT, preferred_element_type=F32)
        out_ref[:, 4 * rows * pair : 4 * rows * (pair + 1)] = product.astype(BF16)
    for copy in sends:
        copy.wait_send()


def mixer_kernel(
    per_group, state_ref, inputs_ref, coef_ref, in_re_ref, in_im_ref, out_re_ref, out_im_ref, skip_ref,
    hidden_ref, gain_ref, w_glu_any, w_out_any, w_group_ref, w_route_ref, ids_ref,
    new_ref, resid_ref, rows_ref, place_ref, active, glu_w, out_w, sems,
):
    step = pl.program_id(0)
    steps = pl.num_programs(0)
    width = inputs_ref.shape[1]
    span = state_ref.shape[2]
    entries = out_re_ref.shape[1]
    channels = width // (span // entries)
    glu_copy = pltpu.make_async_copy(w_glu_any, glu_w, sems.at[0])
    out_copy = pltpu.make_async_copy(w_out_any, out_w, sems.at[1])

    @pl.when(step == 0)
    def _():
        glu_copy.start()
        out_copy.start()

    def iota(shape, axis):
        return lax.broadcasted_iota(jnp.int32, shape, axis)

    spread_out = (iota((entries, span), 1) % entries == iota((entries, span), 0)).astype(BF16)
    mask_out = iota((width, span), 0) // channels == iota((width, span), 1) // entries

    def block(ref):
        tiled = jnp.dot(ref[...].astype(BF16), spread_out, preferred_element_type=F32)
        return jnp.where(mask_out, tiled, 0.0).astype(BF16)

    inputs = inputs_ref[...]
    drive_re = jnp.dot(inputs, block(in_re_ref), preferred_element_type=F32)
    drive_im = jnp.dot(inputs, block(in_im_ref), preferred_element_type=F32)
    bar_re, bar_im = coef_ref[0:1, :], coef_ref[1:2, :]
    coef_re, coef_im = coef_ref[2:3, :], coef_ref[3:4, :]
    old_re, old_im = state_ref[0], state_ref[1]
    new_re = bar_re * old_re - bar_im * old_im + (coef_re * drive_re - coef_im * drive_im)
    new_im = bar_re * old_im + bar_im * old_re + (coef_re * drive_im + coef_im * drive_re)
    new_ref[0] = new_re
    new_ref[1] = new_im
    read = lax.dot_general(new_re.astype(BF16), block(out_re_ref), NT, preferred_element_type=F32)
    read = read - lax.dot_general(new_im.astype(BF16), block(out_im_ref), NT, preferred_element_type=F32)
    mixed = read + skip_ref[...] * inputs.astype(F32)
    active[:, pl.ds(pl.multiple_of(step * width, 128), width)] = jax.nn.gelu(mixed)

    @pl.when(step == steps - 1)
    def _():
        glu_copy.wait()
        out_copy.wait()
        act = active[...]
        gating = jnp.dot(act.astype(BF16), glu_w[...], preferred_element_type=F32)
        glu = (act * jax.nn.sigmoid(gating)).astype(BF16)
        resid = (hidden_ref[...].astype(F32) + jnp.dot(glu, out_w[...], preferred_element_type=F32)).astype(BF16)
        resid_ref[...] = resid
        wide = resid.astype(F32)
        mean = jnp.mean(wide * wide, axis=-1, keepdims=True)
        normed = (wide * lax.rsqrt(mean + 1e-06) * gain_ref[...]).astype(BF16)
        depth = normed.shape[1]
        rows_ref[:, :depth] = normed
        level = lax.dot_general(normed, w_group_ref[...], NT, preferred_element_type=F32)
        logits = lax.dot_general(normed, w_route_ref[...], NT, preferred_element_type=F32)
        count = normed.shape[0]
        lane = iota((count, 128), 1)
        same = (iota((count, count), 0) == iota((count, count), 1)).astype(BF16)
        ids = lax.dot_general(same, ids_ref[...].astype(F32).astype(BF16), NT, preferred_element_type=F32).astype(jnp.int32)
        first, second = ids[:, 0:1], ids[:, 1:2]
        group = first // per_group
        own = jnp.sum(jnp.where(iota(level.shape, 1) == group, level, 0.0), axis=1, keepdims=True)
        scale = 1.0 / jnp.sum(jnp.exp(level - own), axis=1, keepdims=True)
        r0 = jnp.sum(jnp.where(iota(logits.shape, 1) == first, logits, 0.0), axis=1, keepdims=True)
        r1 = jnp.sum(jnp.where(iota(logits.shape, 1) == second, logits, 0.0), axis=1, keepdims=True)
        share = jax.nn.sigmoid(r0 - r1)
        member = lane % per_group
        gate = jnp.where(member == first % per_group, scale * share, 0.0)
        gate = gate + jnp.where(member == second % per_group, scale * (1.0 - share), 0.0)
        high = gate.astype(BF16).astype(F32)
        packed = jnp.where(lane < per_group, high, jnp.where(lane < 2 * per_group, gate - high, 0.0))
        rows_ref[:, depth:] = packed.astype(BF16)
        hits = (lane == group).astype(BF16)
        earlier = (iota((count, count), 1) < iota((count, count), 0)).astype(BF16)
        before = jnp.dot(earlier, hits, preferred_element_type=F32)
        rank = jnp.sum(jnp.where(lane == group, before, 0.0), axis=1, keepdims=True).astype(jnp.int32)
        slots = place_ref.shape[1]
        slot = group * (slots // EXP_GROUPS) + rank
        place_ref[...] = (iota((count, slots), 1) == slot).astype(BF16)


def expert_kernel(
    groups, per_group, rows_ref, place_ref, resid_ref, gate_any, up_any, down_any, out_ref,
    outgoing, tokens, parts, parts_in, sums, sums_in, final, returned, w_gate, w_up, w_down,
    zs, zr, ys, yr, cs, cr, ps, pr, qs, qr, bs, br, w_sems,
):
    grp = lax.axis_index("grp")
    me = lax.axis_index("ep")
    pairs = per_group // 2
    g, p = me // per_group, me % per_group
    q, c = p // 2, p % 2
    depth = resid_ref.shape[1]
    cap = outgoing.shape[1]
    wide = outgoing.shape[2]

    def at(group, pair):
        return (grp, group * per_group + pair * 2 + c)

    mate = (grp, me + 1 - 2 * c)
    others = [(g + i) % groups for i in range(1, groups)]
    mates_q = [(q + j) % pairs for j in range(1, pairs)]
    loads = [
        pltpu.make_async_copy(gate_any.at[0], w_gate, w_sems.at[0]),
        pltpu.make_async_copy(up_any.at[0], w_up, w_sems.at[1]),
        pltpu.make_async_copy(down_any.at[0], w_down, w_sems.at[2]),
    ]
    for load in loads:
        load.start()
    sent = lax.dot_general(place_ref[...], rows_ref[...], TN, preferred_element_type=F32).astype(BF16)
    outgoing[...] = sent.reshape(groups, cap, wide)
    tokens[g, c, q] = outgoing[g]
    greet([at(o, q) for o in others] + [at(g, o) for o in mates_q] + [mate])
    sends = []

    def start(copy):
        copy.start()
        sends.append(copy)

    for target in others:
        start(remote(outgoing.at[target], tokens.at[g, c, q], zs.at[target], zr.at[g], at(target, q)))

    def source(i):
        return (g + groups - i) % groups

    def to_mate(s, pair):
        spot = tokens.at[s, c, pair]
        start(remote(spot, spot, cs.at[s, pair], cr.at[s, pair], mate))

    def stage_a(i):
        s = source(i)
        spot = tokens.at[s, c, q]
        if i > 0:
            remote(spot, spot, zs.at[s], zr.at[s], mate).wait_recv()
        for o in mates_q:
            start(remote(spot, spot, ys.at[s, o], yr.at[s, q], at(g, o)))
        to_mate(s, q)

    def stage_b(i):
        s = source(i)
        for o in mates_q:
            spot = tokens.at[s, c, o]
            remote(spot, spot, ys.at[s, o], yr.at[s, o], mate).wait_recv()
            to_mate(s, o)

    def stage_c(i):
        s = source(i)
        for o in range(pairs):
            spot = tokens.at[s, 1 - c, o]
            remote(spot, spot, cs.at[s, o], cr.at[s, o], mate).wait_recv()
        if i == 0:
            for load in loads:
                load.wait()
        total = per_group * cap
        x = tokens[s].reshape(total, wide)
        rows = x[:, :depth]
        gate = jnp.dot(rows, w_gate[...], preferred_element_type=F32)
        upper = jnp.dot(rows, w_up[...], preferred_element_type=F32)
        inner = (jax.nn.silu(gate) * upper).astype(BF16)
        result = jnp.dot(inner, w_down[...], preferred_element_type=F32).astype(BF16)
        lane = lax.broadcasted_iota(jnp.int32, (total, wide - depth), 1)
        mine = (lane == p) | (lane == p + per_group)
        weight = jnp.sum(jnp.where(mine, x[:, depth:].astype(F32), 0.0), axis=1, keepdims=True)
        parts[s] = (result.astype(F32) * weight).astype(BF16).reshape(2, pairs, cap, depth)
        start(remote(parts.at[s, 1 - c], parts_in.at[s], ps.at[s], pr.at[s], mate))

    def stage_d(i):
        s = source(i)
        spot = parts_in.at[s]
        remote(spot, spot, ps.at[s], pr.at[s], mate).wait_recv()
        sums[s] = (parts[s, c].astype(F32) + parts_in[s].astype(F32)).astype(BF16)
        for o in mates_q:
            start(remote(sums.at[s, o], sums_in.at[s, q], qs.at[s, o], qr.at[s, q], at(g, o)))

    def stage_e(i):
        s = source(i)
        total = sums[s, q].astype(F32)
        for o in mates_q:
            spot = sums_in.at[s, o]
            remote(spot, spot, qs.at[s, o], qr.at[s, o], mate).wait_recv()
            total = total + sums_in[s, o].astype(F32)
        if i == 0:
            returned[g] = total.astype(BF16)
        else:
            final[s] = total.astype(BF16)
            start(remote(final.at[s], returned.at[g], bs.at[s], br.at[g], at(s, q)))

    stage_a(0)
    for t in range(groups):
        stage_b(t)
        if t + 1 < groups:
            stage_a(t + 1)
        stage_c(t)
        stage_d(t)
        if t > 0:
            stage_e(t - 1)
    stage_e(groups - 1)
    for o in others:
        spot = returned.at[o]
        remote(spot, spot, bs.at[o], br.at[o], mate).wait_recv()
    back = returned[...].reshape(groups * cap, depth)
    moe = jnp.dot(place_ref[...], back, preferred_element_type=F32)
    out_ref[...] = (resid_ref[...].astype(F32) + moe).astype(BF16)
    for copy in sends:
        copy.wait_send()


def on_device(
    hidden, state, norm_gain, w_in, lam_re, lam_im, log_step, in_re, in_im, out_re, out_im, skip, w_glu, w_out,
    ffn_gain, w_group, w_route, w_gate, w_up, w_down, route_ids,
):
    rows, depth = hidden.shape
    devices = lax.axis_size("ep")
    chips = devices // 2
    shard = w_in.shape[1]
    dma = pltpu.SemaphoreType.DMA
    inputs = pl.pallas_call(
        functools.partial(gather_kernel, chips),
        out_shape=jax.ShapeDtypeStruct((rows, shard * devices), BF16),
        in_specs=[VMEM] * 3,
        out_specs=VMEM,
        scratch_shapes=[pltpu.VMEM((chips, 2, shard, depth), BF16), pltpu.VMEM((rows, depth), BF16)]
        + [dma((chips // 2, 2))] * 4 + [dma((2, chips // 2, 2))] * 6 + [dma, dma, dma],
        compiler_params=pltpu.CompilerParams(collective_id=0, has_side_effects=True, vmem_limit_bytes=LIMIT),
        name="gather_in",
    )(hidden, norm_gain[None, :], w_in.T)

    groups, entries = lam_re.shape
    width = in_re.shape[2]
    flat = groups * entries
    lr, li = lam_re.reshape(1, flat), lam_im.reshape(1, flat)
    step = jnp.exp(jnp.broadcast_to(log_step[:, None], (groups, entries)).reshape(1, flat))
    magnitude = jnp.exp(lr * step)
    bar_re = magnitude * jnp.cos(li * step)
    bar_im = magnitude * jnp.sin(li * step)
    denom = lr * lr + li * li
    lessened = bar_re - 1.0
    coef = jnp.concatenate(
        [bar_re, bar_im, (lessened * lr + bar_im * li) / denom, (bar_im * lr - lessened * li) / denom], axis=0
    )
    experts = w_route.shape[1]
    per_group = experts // EXP_GROUPS
    cap = 2 * rows // EXP_GROUPS
    block = 128 // width
    span = block * entries
    channels = groups * width
    const = lambda *shape: pl.BlockSpec(shape, lambda i: (0,) * len(shape))
    new_state, resid, packed, place = pl.pallas_call(
        functools.partial(mixer_kernel, per_group),
        grid=(groups // block,),
        out_shape=[
            jax.ShapeDtypeStruct(state.shape, F32),
            jax.ShapeDtypeStruct((rows, depth), BF16),
            jax.ShapeDtypeStruct((rows, depth + 128), BF16),
            jax.ShapeDtypeStruct((rows, EXP_GROUPS * cap), BF16),
        ],
        in_specs=[
            pl.BlockSpec((2, rows, span), lambda i: (0, 0, i)),
            pl.BlockSpec((rows, 128), lambda i: (0, i)),
            pl.BlockSpec((4, span), lambda i: (0, i)),
            pl.BlockSpec((128, entries), lambda i: (i, 0)),
            pl.BlockSpec((128, entries), lambda i: (i, 0)),
            pl.BlockSpec((128, entries), lambda i: (i, 0)),
            pl.BlockSpec((128, entries), lambda i: (i, 0)),
            pl.BlockSpec((1, 128), lambda i: (0, i)),
            const(rows, depth),
            const(1, depth),
            ANY,
            ANY,
            const(EXP_GROUPS, depth),
            const(experts, depth),
            const(TOPK, rows),
        ],
        out_specs=[
            pl.BlockSpec((2, rows, span), lambda i: (0, 0, i)),
            const(rows, depth),
            const(rows, depth + 128),
            const(rows, EXP_GROUPS * cap),
        ],
        scratch_shapes=[
            pltpu.VMEM((rows, channels), F32),
            pltpu.VMEM(w_glu.shape, BF16),
            pltpu.VMEM(w_out.shape, BF16),
            dma((2,)),
        ],
        compiler_params=pltpu.CompilerParams(dimension_semantics=("arbitrary",), vmem_limit_bytes=LIMIT),
        name="mixer",
    )(
        state, inputs, coef, in_re.transpose(0, 2, 1).reshape(channels, entries),
        in_im.transpose(0, 2, 1).reshape(channels, entries),
        out_re.reshape(channels, entries), out_im.reshape(channels, entries), skip[None, :],
        hidden, ffn_gain[None, :], w_glu, w_out, w_group.T, w_route.T, route_ids.T,
    )

    pairs = per_group // 2
    G = EXP_GROUPS
    hidden_out = pl.pallas_call(
        functools.partial(expert_kernel, G, per_group),
        out_shape=jax.ShapeDtypeStruct((rows, depth), BF16),
        in_specs=[VMEM] * 3 + [ANY] * 3,
        out_specs=VMEM,
        scratch_shapes=[
            pltpu.VMEM((G, cap, depth + 128), BF16),
            pltpu.VMEM((G, 2, pairs, cap, depth + 128), BF16),
            pltpu.VMEM((G, 2, pairs, cap, depth), BF16),
            pltpu.VMEM((G, pairs, cap, depth), BF16),
            pltpu.VMEM((G, pairs, cap, depth), BF16),
            pltpu.VMEM((G, pairs, cap, depth), BF16),
            pltpu.VMEM((G, cap, depth), BF16),
            pltpu.VMEM((G, cap, depth), BF16),
            pltpu.VMEM(w_gate.shape[1:], BF16),
            pltpu.VMEM(w_up.shape[1:], BF16),
            pltpu.VMEM(w_down.shape[1:], BF16),
            dma((G,)), dma((G,)), dma((G, pairs)), dma((G, pairs)), dma((G, pairs)), dma((G, pairs)),
            dma((G,)), dma((G,)), dma((G, pairs)), dma((G, pairs)), dma((G,)), dma((G,)), dma((3,)),
        ],
        compiler_params=pltpu.CompilerParams(collective_id=1, has_side_effects=True, vmem_limit_bytes=LIMIT),
        name="experts",
    )(packed, place, resid, w_gate, w_up, w_down)
    return (hidden_out, new_state)


def solution(mesh):
    return jax.shard_map(
        on_device,
        mesh=mesh,
        in_specs=(
            P(("grp", "ep"), None),
            P(None, ("grp", "ep"), None),
            P(),
            P(None, "ep"),
            P(),
            P(),
            P(),
            P(),
            P(),
            P(),
            P(),
            P(),
            P(),
            P(),
            P(),
            P(),
            P(),
            P("ep", None, None),
            P("ep", None, None),
            P("ep", None, None),
            P(("grp", "ep"), None),
        ),
        out_specs=(P(("grp", "ep"), None), P(None, ("grp", "ep"), None)),
        check_vma=False,
    )
```

profile of v0, /device:TPU:0, one launch (start us, length us, event | category | flops | bytes accessed | tf_op | source)
XLA Modules:
  0.0 128.8 jit_solution(12092189522332018498)
XLA Ops:
  0.6 0.7 exp.50
  1.3 0.8 reshape.221
  2.1 0.8 reshape.222
  3.0 0.1 broadcast_in_dim.16
  3.1 0.1 exp.51
  3.2 0.5 cosine_multiply_fusion
  3.7 0.7 pad_maximum_fusion.coef_ref
  4.4 34.2 %gather_in.1.inputs_ref = bf16[128,1024]{1,0:T(8,128)(2,1)} custom-call(bf16[128,2048]{1,0:T(8,128)(2,1)} %hidden_ref.3, f32[1,2048]{1,0:T(1,128)} %bitcast.22, bf16[64,2048]{1,0:T(8,128)(2,1)} %bitcast.19), custom_call_target="tpu_custom_call" | custom-call | tf_op jit(solution)/shard_map/gather_in/pallas_call | solution.py:353
  38.6 14.3 %mixer.1 = (f32[2,128,4096]{2,1,0:T(8,128)}, bf16[128,2048]{1,0:T(8,128)(2,1)}, bf16[128,2176]{1,0:T(8,128)(2,1)}, bf16[128,256]{1,0:T(8,128)(2,1)}) custom-call(f32[2,128,4096]{2,1,0:T(8,128)} %state_ref.1, bf16[128,1024]{1,0:T(8,128)(2,1)} %gather_in.1.inputs_ref, f32[4,4096]{1,0:T(4,128)} %pad_maximum_fusion.coef_ref, f32[1024,64]{1,0:T(8,128)} %bitcast.15, ...), custom_call_target="tpu_custom_call" | custom-call | tf_op jit(solution)/shard_map/mixer/pallas_call | solution.py:384
  52.9 74.0 %experts.1 = bf16[128,2048]{1,0:T(8,128)(2,1)} custom-call(bf16[128,2176]{1,0:T(8,128)(2,1)} %get-tuple-element.6.rows_ref, bf16[128,256]{1,0:T(8,128)(2,1)} %get-tuple-element.7.place_ref, bf16[128,2048]{1,0:T(8,128)(2,1)} %get-tuple-element.8.resid_ref, bf16[1,2048,512]{2,1,0:T(8,128)(2,1)} %gate_any.1, bf16[1,2048,512]{2,1,0:T(8,128)(2,1)} %up_any.1, ...), custom_call_target="tpu_custom_call" | custom-call | tf_op jit(solution)/shard_map/experts/pallas_call | solution.py:433
  126.9 1.9 %copy.24 = bf16[128,2048]{1,0:T(8,128)(2,1)} copy(bf16[128,2048]{1,0:T(8,128)(2,1)} %experts.1) | data formatting | bytes 1048576
where the time goes:
time: 129 us
  Pallas kernels  123 us (95%)
  local copies, waits for them, and re-layouts  4.39 us (3%)
    pallas_call x1, Pallas kernels, on_device(): pl.pallas_call(functools.partial(expert_kernel, G, per_group), out_shape=...  74 us
    pallas_call x1, Pallas kernels, on_device(): pl.pallas_call(functools.partial(gather_kernel, chips), out_shape=jax.Sha...  34.2 us
    pallas_call x1, Pallas kernels, on_device(): pl.pallas_call(functools.partial(mixer_kernel, per_group), grid=(groups /...  14.3 us

commit v1 on v0

v1 whole, which is shorter than its diff:
```python
import functools

import jax
import jax.numpy as jnp
from jax import lax
from jax.experimental import pallas as pl
from jax.experimental.pallas import tpu as pltpu
from jax.sharding import PartitionSpec as P

EXP_GROUPS = 4
TOPK = 2
MESH = pl.DeviceIdType.MESH
VMEM = pl.BlockSpec(memory_space=pltpu.VMEM)
ANY = pl.BlockSpec(memory_space=pl.ANY)
F32 = jnp.float32
BF16 = jnp.bfloat16
NT = (((1,), (1,)), ((), ()))
TN = (((0,), (0,)), ((), ()))
LIMIT = 60 * 1024 * 1024
FRONT_LIMIT = 44 * 1024 * 1024


def remote(src, dst, send_sem, recv_sem, device):
    return pltpu.make_async_remote_copy(
        src_ref=src, dst_ref=dst, send_sem=send_sem, recv_sem=recv_sem, device_id=device, device_id_type=MESH
    )


def greet(peers):
    barrier = pltpu.get_barrier_semaphore()
    for peer in peers:
        pl.semaphore_signal(barrier, inc=1, device_id=peer, device_id_type=MESH)
    pl.semaphore_wait(barrier, len(peers))


def front_kernel(
    chips, per_group, hidden_any, gain_ref, w_any, state_any, lam_re_ref, lam_im_ref, step_ref, in_re_any, in_im_any,
    out_re_any, out_im_any, skip_ref, ffn_gain_ref, w_glu_any, w_out_any, w_group_ref, w_route_ref, ids_ref,
    new_any, resid_ref, rows_ref, place_ref,
    held, hidden, state, in_re, in_im, out_re, out_im, glu_w, out_w, normed, coef, active, gating,
    zs, zr, ys, yr, xs, xr, ds, dr, own_s, own_r, load_sems, state_sems, new_sems,
):
    grp = lax.axis_index("grp")
    me = lax.axis_index("ep")
    chip, core = me // 2, me % 2
    lines = chips // 2
    line, y = chip // 2, chip % 2
    side = grp % 2
    shard, depth = w_any.shape
    entries = lam_re_ref.shape[1]
    unit = 128 // (2 * shard)
    blocks = chips // unit
    span = state.shape[2] // blocks
    channels = 128 // (span // entries)

    def at(row, column):
        return (grp, (row * 2 + column) * 2 + core)

    mate = (grp, me + 1 - 2 * core)
    across = (grp + 1 - 2 * side, me)
    beside = at(line, 1 - y)
    after = lines - 1 - line
    longer = (after - line + lines - 1) // lines
    short = line * longer + after * (1 - longer)

    def near(k):
        past = (k + 2 * lines - 2 * short) // (2 * lines)
        paired = (k // 2 + 1) * (1 - 2 * (k % 2))
        single = (k - short + 1) * (2 * longer - 1)
        return line + paired * (1 - past) + single * past

    order = [near(k) for k in range(lines - 1)]
    third = depth // 3 // 128 * 128
    middle = depth - 2 * third
    cols = [
        pl.ds(pl.multiple_of(side * (depth - third), 128), third),
        pl.ds(third, middle),
        pl.ds(pl.multiple_of((1 - side) * (depth - third), 128), third),
    ]
    sends = []

    def start(copy):
        copy.start()
        sends.append(copy)

    def column(j):
        return pl.ds(pl.multiple_of(j * span, 128), span)

    own = pltpu.make_async_copy(w_any, held.at[chip, core], load_sems.at[0])
    own.start()
    loads = [
        pltpu.make_async_copy(src, dst, load_sems.at[1 + i])
        for i, (src, dst) in enumerate([
            (hidden_any, hidden), (in_re_any, in_re), (in_im_any, in_im), (out_re_any, out_re), (out_im_any, out_im),
            (w_glu_any, glu_w), (w_out_any, out_w),
        ])
    ]
    for load in loads[:1]:
        load.start()
    greet([at(o, y) for o in order] + [beside, mate, across])
    own.wait()
    for p in range(2):
        spot = held.at[chip, core, :, cols[p]]
        start(remote(spot, spot, ys.at[line, p], yr.at[line, p], beside))
        for o in order:
            start(remote(spot, spot, zs.at[o, p], zr.at[line, p], at(o, y)))
    spot = held.at[chip, core]
    start(remote(spot, spot, own_s, own_r, mate))
    for load in loads[1:]:
        load.start()
    block_loads = [
        pltpu.make_async_copy(state_any.at[:, :, pl.ds(j * span, span)], state.at[:, :, pl.ds(j * span, span)], state_sems.at[j])
        for j in range(blocks)
    ]
    for load in block_loads:
        load.start()

    def iota(shape, axis):
        return lax.broadcasted_iota(jnp.int32, shape, axis)

    loads[0].wait()
    wide = hidden[...].astype(F32)
    mean = jnp.mean(wide * wide, axis=-1, keepdims=True)
    normed[...] = (wide * lax.rsqrt(mean + 1e-06) * gain_ref[...]).astype(BF16)

    groups = lam_re_ref.shape[0]
    lr, li = lam_re_ref[...], lam_im_ref[...]
    diagonal = iota((groups, groups), 0) == iota((groups, groups), 1)
    step = jnp.exp(jnp.sum(jnp.where(diagonal, step_ref[...], 0.0), axis=1, keepdims=True))
    magnitude = jnp.exp(lr * step)
    bar_re = magnitude * jnp.cos(li * step)
    bar_im = magnitude * jnp.sin(li * step)
    denom = lr * lr + li * li
    lessened = bar_re - 1.0
    coef[0] = bar_re
    coef[1] = bar_im
    coef[2] = (lessened * lr + bar_im * li) / denom
    coef[3] = (bar_im * lr - lessened * li) / denom
    for load in loads[1:5]:
        load.wait()
    for load in block_loads:
        load.wait()
    gating[...] = jnp.zeros_like(gating)

    spread = iota((entries, span), 1) % entries == iota((entries, span), 0)
    mask = iota((128, span), 0) // channels == iota((128, span), 1) // entries
    pick = iota((span // entries, span), 0) == iota((span // entries, span), 1) // entries

    def expand(ref, j):
        part = ref[pl.ds(pl.multiple_of(j * 128, 128), 128), :].astype(BF16)
        tiled = jnp.dot(part, spread.astype(BF16), preferred_element_type=F32)
        return jnp.where(mask, tiled, 0.0).astype(BF16)

    def mix(j):
        block = held[pl.ds(j * unit, unit)].reshape(128, depth)
        inputs = lax.dot_general(normed[...], block, NT, preferred_element_type=F32).astype(BF16)
        drive_re = jnp.dot(inputs, expand(in_re, j), preferred_element_type=F32)
        drive_im = jnp.dot(inputs, expand(in_im, j), preferred_element_type=F32)
        per = span // entries
        rows = coef[:, pl.ds(pl.multiple_of(j * per, per), per), :].reshape(4 * per, entries)
        tiled = jnp.dot(rows, spread.astype(F32), precision=lax.Precision.HIGHEST, preferred_element_type=F32)
        line_of = [
            jnp.sum(jnp.where(pick, tiled[i * per : (i + 1) * per], 0.0), axis=0, keepdims=True) for i in range(4)
        ]
        old_re, old_im = state[0, :, column(j)], state[1, :, column(j)]
        new_re = line_of[0] * old_re - line_of[1] * old_im + (line_of[2] * drive_re - line_of[3] * drive_im)
        new_im = line_of[0] * old_im + line_of[1] * old_re + (line_of[2] * drive_im + line_of[3] * drive_re)
        state[0, :, column(j)] = new_re
        state[1, :, column(j)] = new_im
        read = lax.dot_general(new_re.astype(BF16), expand(out_re, j), NT, preferred_element_type=F32)
        read = read - lax.dot_general(new_im.astype(BF16), expand(out_im, j), NT, preferred_element_type=F32)
        lanes = pl.ds(pl.multiple_of(j * 128, 128), 128)
        act = jax.nn.gelu(read + skip_ref[:, lanes] * inputs.astype(F32))
        active[:, lanes] = act
        gating[...] += jnp.dot(act.astype(BF16), glu_w[lanes, :], preferred_element_type=F32)
        pltpu.make_async_copy(state.at[:, :, column(j)], new_any.at[:, :, column(j)], new_sems.at[j]).start()

    def place(item):
        kind, k = item
        if kind == 0:
            return order[k] * 2 + y
        return (line if k < 0 else order[k]) * 2 + 1 - y

    def take(item, p):
        kind, k = item
        s = line if k < 0 else order[k]
        spot = held.at[place(item), core, :, cols[p]]
        if kind == 0:
            remote(spot, spot, zs.at[s, p], zr.at[s, p], mate).wait_recv()
            start(remote(spot, spot, ys.at[s, p], yr.at[s, p], beside))
        else:
            remote(spot, spot, ys.at[s, p], yr.at[s, p], mate).wait_recv()
        if p == 0:
            start(remote(spot, spot, xs.at[place(item)], xr.at[place(item)], across))
        start(remote(spot, spot, ds.at[place(item), p], dr.at[place(item), p], mate))

    def take_x(item):
        spot = held.at[place(item), core, :, cols[2]]
        remote(spot, spot, xs.at[place(item)], xr.at[place(item)], mate).wait_recv()
        start(remote(spot, spot, ds.at[place(item), 2], dr.at[place(item), 2], mate))

    def settle(item):
        for p in range(3):
            spot = held.at[place(item), 1 - core, :, cols[p]]
            remote(spot, spot, ds.at[place(item), p], dr.at[place(item), p], mate).wait_recv()

    items = [(1, -1)]
    for k in range(lines):
        if k < lines - 1:
            items.append((0, k))
        if k > 0:
            items.append((1, k - 1))
    spot = held.at[chip, 1 - core]
    remote(spot, spot, own_s, own_r, mate).wait_recv()
    loads[5].wait()
    if unit == 1:
        mix(chip)
    for item in items:
        take(item, 0)
    ready = {-1: 1}
    for at_ in range(len(items) + 1):
        if at_ < len(items):
            take(items[at_], 1)
            if at_ == 0:
                continue
        take_x(items[at_ - 1])
        settle(items[at_ - 1])
        kind, k = items[at_ - 1]
        if unit == 1:
            mix(place(items[at_ - 1]))
        else:
            ready[k] = ready.get(k, 0) + 1
            if ready[k] == unit:
                mix(line if k < 0 else order[k])
    loads[6].wait()

    act = active[...]
    glu = (act * jax.nn.sigmoid(gating[...])).astype(BF16)
    resid = (hidden[...].astype(F32) + jnp.dot(glu, out_w[...], preferred_element_type=F32)).astype(BF16)
    resid_ref[...] = resid
    wide = resid.astype(F32)
    mean = jnp.mean(wide * wide, axis=-1, keepdims=True)
    second_normed = (wide * lax.rsqrt(mean + 1e-06) * ffn_gain_ref[...]).astype(BF16)
    rows_ref[:, :depth] = second_normed
    level = lax.dot_general(second_normed, w_group_ref[...], NT, preferred_element_type=F32)
    logits = lax.dot_general(second_normed, w_route_ref[...], NT, preferred_element_type=F32)
    count = second_normed.shape[0]
    lane = iota((count, 128), 1)
    same = (iota((count, count), 0) == iota((count, count), 1)).astype(BF16)
    ids = lax.dot_general(same, ids_ref[...].astype(F32).astype(BF16), NT, preferred_element_type=F32).astype(jnp.int32)
    first, second = ids[:, 0:1], ids[:, 1:2]
    group = first // per_group
    chosen = jnp.sum(jnp.where(iota(level.shape, 1) == group, level, 0.0), axis=1, keepdims=True)
    scale = 1.0 / jnp.sum(jnp.exp(level - chosen), axis=1, keepdims=True)
    r0 = jnp.sum(jnp.where(iota(logits.shape, 1) == first, logits, 0.0), axis=1, keepdims=True)
    r1 = jnp.sum(jnp.where(iota(logits.shape, 1) == second, logits, 0.0), axis=1, keepdims=True)
    share = jax.nn.sigmoid(r0 - r1)
    member = lane % per_group
    gate = jnp.where(member == first % per_group, scale * share, 0.0)
    gate = gate + jnp.where(member == second % per_group, scale * (1.0 - share), 0.0)
    high = gate.astype(BF16).astype(F32)
    packed = jnp.where(lane < per_group, high, jnp.where(lane < 2 * per_group, gate - high, 0.0))
    rows_ref[:, depth:] = packed.astype(BF16)
    hits = (lane == group).astype(BF16)
    earlier = (iota((count, count), 1) < iota((count, count), 0)).astype(BF16)
    before = jnp.dot(earlier, hits, preferred_element_type=F32)
    rank = jnp.sum(jnp.where(lane == group, before, 0.0), axis=1, keepdims=True).astype(jnp.int32)
    slots = place_ref.shape[1]
    slot = group * (slots // EXP_GROUPS) + rank
    place_ref[...] = (iota((count, slots), 1) == slot).astype(BF16)
    for j in range(blocks):
        columns = pl.ds(j * span, span)
        pltpu.make_async_copy(state.at[:, :, columns], new_any.at[:, :, columns], new_sems.at[j]).wait()
    for copy in sends:
        copy.wait_send()


def expert_kernel(
    groups, per_group, rows_ref, place_ref, resid_ref, gate_any, up_any, down_any, out_ref,
    outgoing, tokens, parts, parts_in, sums, sums_in, final, returned, w_gate, w_up, w_down,
    zs, zr, ys, yr, cs, cr, ps, pr, qs, qr, bs, br, w_sems,
):
    grp = lax.axis_index("grp")
    me = lax.axis_index("ep")
    pairs = per_group // 2
    g, p = me // per_group, me % per_group
    q, c = p // 2, p % 2
    depth = resid_ref.shape[1]
    cap = outgoing.shape[1]
    wide = outgoing.shape[2]

    def at(group, pair):
        return (grp, group * per_group + pair * 2 + c)

    mate = (grp, me + 1 - 2 * c)
    others = [(g + i) % groups for i in range(1, groups)]
    mates_q = [(q + j) % pairs for j in range(1, pairs)]
    loads = [
        pltpu.make_async_copy(gate_any.at[0], w_gate, w_sems.at[0]),
        pltpu.make_async_copy(up_any.at[0], w_up, w_sems.at[1]),
        pltpu.make_async_copy(down_any.at[0], w_down, w_sems.at[2]),
    ]
    for load in loads:
        load.start()
    sent = lax.dot_general(place_ref[...], rows_ref[...], TN, preferred_element_type=F32).astype(BF16)
    outgoing[...] = sent.reshape(groups, cap, wide)
    tokens[g, c, q] = outgoing[g]
    greet([at(o, q) for o in others] + [at(g, o) for o in mates_q] + [mate])
    sends = []

    def start(copy):
        copy.start()
        sends.append(copy)

    for target in others:
        start(remote(outgoing.at[target], tokens.at[g, c, q], zs.at[target], zr.at[g], at(target, q)))

    def source(i):
        return (g + groups - i) % groups

    def to_mate(s, pair):
        spot = tokens.at[s, c, pair]
        start(remote(spot, spot, cs.at[s, pair], cr.at[s, pair], mate))

    def stage_a(i):
        s = source(i)
        spot = tokens.at[s, c, q]
        if i > 0:
            remote(spot, spot, zs.at[s], zr.at[s], mate).wait_recv()
        for o in mates_q:
            start(remote(spot, spot, ys.at[s, o], yr.at[s, q], at(g, o)))
        to_mate(s, q)

    def stage_b(i):
        s = source(i)
        for o in mates_q:
            spot = tokens.at[s, c, o]
            remote(spot, spot, ys.at[s, o], yr.at[s, o], mate).wait_recv()
            to_mate(s, o)

    def stage_c(i):
        s = source(i)
        for o in range(pairs):
            spot = tokens.at[s, 1 - c, o]
            remote(spot, spot, cs.at[s, o], cr.at[s, o], mate).wait_recv()
        if i == 0:
            for load in loads:
                load.wait()
        total = per_group * cap
        x = tokens[s].reshape(total, wide)
        rows = x[:, :depth]
        gate = jnp.dot(rows, w_gate[...], preferred_element_type=F32)
        upper = jnp.dot(rows, w_up[...], preferred_element_type=F32)
        inner = (jax.nn.silu(gate) * upper).astype(BF16)
        result = jnp.dot(inner, w_down[...], preferred_element_type=F32).astype(BF16)
        lane = lax.broadcasted_iota(jnp.int32, (total, wide - depth), 1)
        mine = (lane == p) | (lane == p + per_group)
        weight = jnp.sum(jnp.where(mine, x[:, depth:].astype(F32), 0.0), axis=1, keepdims=True)
        parts[s] = (result.astype(F32) * weight).astype(BF16).reshape(2, pairs, cap, depth)
        start(remote(parts.at[s, 1 - c], parts_in.at[s], ps.at[s], pr.at[s], mate))

    def stage_d(i):
        s = source(i)
        spot = parts_in.at[s]
        remote(spot, spot, ps.at[s], pr.at[s], mate).wait_recv()
        sums[s] = (parts[s, c].astype(F32) + parts_in[s].astype(F32)).astype(BF16)
        for o in mates_q:
            start(remote(sums.at[s, o], sums_in.at[s, q], qs.at[s, o], qr.at[s, q], at(g, o)))

    def stage_e(i):
        s = source(i)
        total = sums[s, q].astype(F32)
        for o in mates_q:
            spot = sums_in.at[s, o]
            remote(spot, spot, qs.at[s, o], qr.at[s, o], mate).wait_recv()
            total = total + sums_in[s, o].astype(F32)
        if i == 0:
            returned[g] = total.astype(BF16)
        else:
            final[s] = total.astype(BF16)
            start(remote(final.at[s], returned.at[g], bs.at[s], br.at[g], at(s, q)))

    stage_a(0)
    for t in range(groups):
        stage_b(t)
        if t + 1 < groups:
            stage_a(t + 1)
        stage_c(t)
        stage_d(t)
        if t > 0:
            stage_e(t - 1)
    stage_e(groups - 1)
    for o in others:
        spot = returned.at[o]
        remote(spot, spot, bs.at[o], br.at[o], mate).wait_recv()
    back = returned[...].reshape(groups * cap, depth)
    moe = jnp.dot(place_ref[...], back, preferred_element_type=F32)
    out_ref[...] = (resid_ref[...].astype(F32) + moe).astype(BF16)
    for copy in sends:
        copy.wait_send()


def on_device(
    hidden, state, norm_gain, w_in, lam_re, lam_im, log_step, in_re, in_im, out_re, out_im, skip, w_glu, w_out,
    ffn_gain, w_group, w_route, w_gate, w_up, w_down, route_ids,
):
    rows, depth = hidden.shape
    devices = lax.axis_size("ep")
    chips = devices // 2
    shard = w_in.shape[1]
    dma = pltpu.SemaphoreType.DMA
    groups, entries = lam_re.shape
    width = in_re.shape[2]
    channels = groups * width
    lines = chips // 2
    blocks = channels // 128
    experts = w_route.shape[1]
    per_group = experts // EXP_GROUPS
    cap = 2 * rows // EXP_GROUPS
    new_state, resid, packed, place = pl.pallas_call(
        functools.partial(front_kernel, chips, per_group),
        out_shape=[
            jax.ShapeDtypeStruct(state.shape, F32),
            jax.ShapeDtypeStruct((rows, depth), BF16),
            jax.ShapeDtypeStruct((rows, depth + 128), BF16),
            jax.ShapeDtypeStruct((rows, EXP_GROUPS * cap), BF16),
        ],
        in_specs=[ANY, VMEM, ANY, ANY] + [VMEM] * 3 + [ANY] * 4 + [VMEM] * 2 + [ANY] * 2 + [VMEM] * 3,
        out_specs=[ANY] + [VMEM] * 3,
        scratch_shapes=[
            pltpu.VMEM((chips, 2, shard, depth), BF16),
            pltpu.VMEM((rows, depth), BF16),
            pltpu.VMEM(state.shape, F32),
        ] + [pltpu.VMEM((channels, entries), F32)] * 4 + [
            pltpu.VMEM(w_glu.shape, BF16),
            pltpu.VMEM(w_out.shape, BF16),
            pltpu.VMEM((rows, depth), BF16),
            pltpu.VMEM((4, groups, entries), F32),
            pltpu.VMEM((rows, channels), F32),
            pltpu.VMEM((rows, channels), F32),
        ] + [dma((lines, 2))] * 4 + [dma((chips,))] * 2 + [dma((chips, 3))] * 2
        + [dma, dma, dma((8,)), dma((blocks,)), dma((blocks,))],
        compiler_params=pltpu.CompilerParams(collective_id=0, has_side_effects=True, vmem_limit_bytes=FRONT_LIMIT),
        name="front",
    )(
        hidden, norm_gain[None, :], w_in.T, state, lam_re, lam_im, log_step[None, :],
        in_re.transpose(0, 2, 1).reshape(channels, entries), in_im.transpose(0, 2, 1).reshape(channels, entries),
        out_re.reshape(channels, entries), out_im.reshape(channels, entries), skip[None, :], ffn_gain[None, :],
        w_glu, w_out, w_group.T, w_route.T, route_ids.T,
    )

    pairs = per_group // 2
    G = EXP_GROUPS
    hidden_out = pl.pallas_call(
        functools.partial(expert_kernel, G, per_group),
        out_shape=jax.ShapeDtypeStruct((rows, depth), BF16),
        in_specs=[VMEM] * 3 + [ANY] * 3,
        out_specs=VMEM,
        scratch_shapes=[
            pltpu.VMEM((G, cap, depth + 128), BF16),
            pltpu.VMEM((G, 2, pairs, cap, depth + 128), BF16),
            pltpu.VMEM((G, 2, pairs, cap, depth), BF16),
            pltpu.VMEM((G, pairs, cap, depth), BF16),
            pltpu.VMEM((G, pairs, cap, depth), BF16),
            pltpu.VMEM((G, pairs, cap, depth), BF16),
            pltpu.VMEM((G, cap, depth), BF16),
            pltpu.VMEM((G, cap, depth), BF16),
            pltpu.VMEM(w_gate.shape[1:], BF16),
            pltpu.VMEM(w_up.shape[1:], BF16),
            pltpu.VMEM(w_down.shape[1:], BF16),
            dma((G,)), dma((G,)), dma((G, pairs)), dma((G, pairs)), dma((G, pairs)), dma((G, pairs)),
            dma((G,)), dma((G,)), dma((G, pairs)), dma((G, pairs)), dma((G,)), dma((G,)), dma((3,)),
        ],
        compiler_params=pltpu.CompilerParams(collective_id=1, has_side_effects=True, vmem_limit_bytes=LIMIT),
        name="experts",
    )(packed, place, resid, w_gate, w_up, w_down)
    return (hidden_out, new_state)


def solution(mesh):
    return jax.shard_map(
        on_device,
        mesh=mesh,
        in_specs=(
            P(("grp", "ep"), None),
            P(None, ("grp", "ep"), None),
            P(),
            P(None, "ep"),
            P(),
            P(),
            P(),
            P(),
            P(),
            P(),
            P(),
            P(),
            P(),
            P(),
            P(),
            P(),
            P(),
            P("ep", None, None),
            P("ep", None, None),
            P("ep", None, None),
            P(("grp", "ep"), None),
        ),
        out_specs=(P(("grp", "ep"), None), P(None, ("grp", "ep"), None)),
        check_vma=False,
    )
```

time: 129 us -> 141 us (1.093)
  the two profiles are of different devices: /device:TPU:0 before, /device:TPU:7 now
where the time goes in v1:
time: 141 us; the launch traced here: 140 us
  Pallas kernels  116 us (82%)
  local copies, waits for them, and re-layouts  23 us (16%)
    pallas_call x1, Pallas kernels, on_device(): pl.pallas_call(functools.partial(expert_kernel, G, per_group), out_shape=...  75.8 us
    pallas_call x1, Pallas kernels, on_device(): pl.pallas_call(functools.partial(front_kernel, chips, per_group), out_sha...  40.5 us
    unnamed x40, local copies, waits for them, and re-layouts  23 us

profile of v1, /device:TPU:7, one launch (start us, length us, event | category | flops | bytes accessed | tf_op | source)
XLA Modules:
  0.0 140.0 jit_solution(12952504367848995480)
XLA Ops:
  0.6 0.0 copy-start
  0.6 1.6 %copy-done = bf16[1024,1024]{1,0:T(8,128)(2,1)S(1)} copy-done((bf16[1024,1024]{1,0:T(8,128)(2,1)S(1)}, bf16[1024,1024]{1,0:T(8,128)(2,1)}, u32[]{:S(2)}) %copy-start) | copy-done | bytes 2097176
  2.2 0.0 copy-start.2
  2.2 1.0 copy-done.2
  3.3 0.0 copy-start.3
  3.3 1.0 copy-done.3
  4.3 0.0 copy-start.4
  4.3 1.0 copy-done.4
  5.4 0.0 copy-start.5
  5.4 1.0 copy-done.5
  6.4 0.0 copy-start.6
  6.4 1.0 copy-done.6
  7.4 0.0 copy-start.8
  7.4 0.9 copy-done.8
  8.4 0.0 copy-start.10
  8.4 0.8 copy-done.10
  9.2 0.0 copy-start.11
  9.2 0.8 copy-done.11
  10.0 0.0 copy-start.12
  10.0 0.8 copy-done.12
  10.7 0.0 copy-start.13
  10.8 0.7 copy-done.13
  11.5 0.0 copy-start.14
  11.5 0.7 copy-done.14
  12.2 0.0 copy-start.15
  12.2 0.7 copy-done.15
  12.9 0.0 copy-start.16
  12.9 0.7 copy-done.16
  13.5 0.0 copy-start.17
  13.6 0.7 copy-done.17
  14.2 0.0 copy-start.18
  14.2 0.7 copy-done.18
  14.9 40.5 %front.1 = (f32[2,128,4096]{2,1,0:T(8,128)}, bf16[128,2048]{1,0:T(8,128)(2,1)S(1)}, bf16[128,2176]{1,0:T(8,128)(2,1)S(1)}, bf16[128,256]{1,0:T(8,128)(2,1)S(1)}) custom-call(bf16[128,2048]{1,0:T(8,128)(2,1)S(1)} %copy-done.2, f32[1,2048]{1,0:T(1,128)S(1)} %bitcast.23, bf16[64,2048]{1,0:T(8,128)(2,1)S(1)} %bitcast.20, f32[2,128,4096]{2,1,0:T(8,128)} %state_any.1, ...), custom_call_target="tpu_custom_call" | custom-call | tf_op jit(solution)/shard_map/front/pallas_call | solution.py:420
  55.4 0.0 copy-start.1
  55.4 0.8 copy-done.1
  56.2 0.0 copy-start.7
  56.2 0.8 copy-done.7
  57.0 0.0 copy-start.9
  57.0 0.6 copy-done.9
  57.6 75.8 %experts.1 = bf16[128,2048]{1,0:T(8,128)(2,1)} custom-call(bf16[128,2176]{1,0:T(8,128)(2,1)} %copy-done.1, bf16[128,256]{1,0:T(8,128)(2,1)} %copy-done.9, bf16[128,2048]{1,0:T(8,128)(2,1)} %copy-done.7, bf16[1,2048,512]{2,1,0:T(8,128)(2,1)} %gate_any.1, bf16[1,2048,512]{2,1,0:T(8,128)(2,1)} %up_any.1, bf16[1,512,2048]{2,1,0:T(8,128)(2,1)} %down_any.1), custom_call_target="tpu_custom_call" | custom-call | tf_op jit(solution)/shard_map/experts/pallas_call | solution.py:454
  133.4 1.9 %copy.25 = bf16[128,2048]{1,0:T(8,128)(2,1)} copy(bf16[128,2048]{1,0:T(8,128)(2,1)} %experts.1) | data formatting | bytes 1048576
  135.3 4.7 %copy.26 = f32[2,128,4096]{2,1,0:T(8,128)} copy(f32[2,128,4096]{2,1,0:T(8,128)} %get-tuple-element.13) | data formatting | bytes 8388608
Async XLA Ops:
  0.6 1.6 %copy-start = (bf16[1024,1024]{1,0:T(8,128)(2,1)S(1)}, bf16[1024,1024]{1,0:T(8,128)(2,1)}, u32[]{:S(2)}) copy-start(bf16[1024,1024]{1,0:T(8,128)(2,1)} %w_glu_any.1) | copy-start | bytes 6291460
  2.2 1.0 copy-start.2
  3.3 1.0 copy-start.3
  4.3 1.0 copy-start.4
  5.4 1.0 copy-start.5
  6.4 1.0 copy-start.6
  7.4 0.9 copy-start.8
  8.4 0.8 copy-start.10
  9.2 0.8 copy-start.11
  10.0 0.8 copy-start.12
  10.7 0.7 copy-start.13
  11.5 0.7 copy-start.14
  12.2 0.7 copy-start.15
  12.9 0.7 copy-start.16
  13.5 0.7 copy-start.17
  14.2 0.7 copy-start.18
  55.4 0.8 copy-start.1
  56.2 0.8 copy-start.7
  57.0 0.6 copy-start.9

commit v2 on v1

--- a/solution.py
+++ b/solution.py
@@ -16,8 +16,8 @@
 BF16 = jnp.bfloat16
 NT = (((1,), (1,)), ((), ()))
 TN = (((0,), (0,)), ((), ()))
-LIMIT = 60 * 1024 * 1024
-FRONT_LIMIT = 44 * 1024 * 1024
+LIMIT = 57 * 1024 * 1024
+FINISH_LIMIT = 16 * 1024 * 1024
 
 
 def remote(src, dst, send_sem, recv_sem, device):
@@ -33,12 +33,22 @@
     pl.semaphore_wait(barrier, len(peers))
 
 
-def front_kernel(
-    chips, per_group, hidden_any, gain_ref, w_any, state_any, lam_re_ref, lam_im_ref, step_ref, in_re_any, in_im_any,
+def nearest(spot, count, k):
+    after = count - 1 - spot
+    longer = (after - spot + count - 1) // count
+    short = spot * longer + after * (1 - longer)
+    past = (k + 2 * count - 2 * short) // (2 * count)
+    paired = (k // 2 + 1) * (1 - 2 * (k % 2))
+    single = (k - short + 1) * (2 * longer - 1)
+    return spot + paired * (1 - past) + single * past
+
+
+def front(
+    chips, per_group, sends, hidden_any, gain_ref, w_any, state_any, lam_re_ref, lam_im_ref, step_ref, in_re_any, in_im_any,
     out_re_any, out_im_any, skip_ref, ffn_gain_ref, w_glu_any, w_out_any, w_group_ref, w_route_ref, ids_ref,
-    new_any, resid_ref, rows_ref, place_ref,
-    held, hidden, state, in_re, in_im, out_re, out_im, glu_w, out_w, normed, coef, active, gating,
-    zs, zr, ys, yr, xs, xr, ds, dr, own_s, own_r, load_sems, state_sems, new_sems,
+    state, resid_ref, place_ref, rows_ref,
+    held, hidden, in_re, in_im, out_re, out_im, glu_w, out_w, normed, coef, active, gating,
+    zs, zr, ys, yr, xs, xr, ds, dr, own_s, own_r, load_sems, state_sems, meet, expert_loads,
 ):
     grp = lax.axis_index("grp")
     me = lax.axis_index("ep")
@@ -59,17 +69,7 @@
     mate = (grp, me + 1 - 2 * core)
     across = (grp + 1 - 2 * side, me)
     beside = at(line, 1 - y)
-    after = lines - 1 - line
-    longer = (after - line + lines - 1) // lines
-    short = line * longer + after * (1 - longer)
-
-    def near(k):
-        past = (k + 2 * lines - 2 * short) // (2 * lines)
-        paired = (k // 2 + 1) * (1 - 2 * (k % 2))
-        single = (k - short + 1) * (2 * longer - 1)
-        return line + paired * (1 - past) + single * past
-
-    order = [near(k) for k in range(lines - 1)]
+    order = [nearest(line, lines, k) for k in range(lines - 1)]
     third = depth // 3 // 128 * 128
     middle = depth - 2 * third
     cols = [
@@ -77,7 +77,6 @@
         pl.ds(third, middle),
         pl.ds(pl.multiple_of((1 - side) * (depth - third), 128), third),
     ]
-    sends = []
 
     def start(copy):
         copy.start()
@@ -97,7 +96,7 @@
     ]
     for load in loads[:1]:
         load.start()
-    greet([at(o, y) for o in order] + [beside, mate, across])
+    meet([at(o, y) for o in order] + [beside, mate, across])
     own.wait()
     for p in range(2):
         spot = held.at[chip, core, :, cols[p]]
@@ -112,7 +111,7 @@
         pltpu.make_async_copy(state_any.at[:, :, pl.ds(j * span, span)], state.at[:, :, pl.ds(j * span, span)], state_sems.at[j])
         for j in range(blocks)
     ]
-    for load in block_loads:
+    for load in block_loads + expert_loads:
         load.start()
 
     def iota(shape, axis):
@@ -173,7 +172,6 @@
         act = jax.nn.gelu(read + skip_ref[:, lanes] * inputs.astype(F32))
         active[:, lanes] = act
         gating[...] += jnp.dot(act.astype(BF16), glu_w[lanes, :], preferred_element_type=F32)
-        pltpu.make_async_copy(state.at[:, :, column(j)], new_any.at[:, :, column(j)], new_sems.at[j]).start()
 
     def place(item):
         kind, k = item
@@ -268,86 +266,75 @@
     slots = place_ref.shape[1]
     slot = group * (slots // EXP_GROUPS) + rank
     place_ref[...] = (iota((count, slots), 1) == slot).astype(BF16)
-    for j in range(blocks):
-        columns = pl.ds(j * span, span)
-        pltpu.make_async_copy(state.at[:, :, columns], new_any.at[:, :, columns], new_sems.at[j]).wait()
-    for copy in sends:
-        copy.wait_send()
-
-
-def expert_kernel(
-    groups, per_group, rows_ref, place_ref, resid_ref, gate_any, up_any, down_any, out_ref,
-    outgoing, tokens, parts, parts_in, sums, sums_in, final, returned, w_gate, w_up, w_down,
-    zs, zr, ys, yr, cs, cr, ps, pr, qs, qr, bs, br, w_sems,
+
+
+def experts(
+    groups, per_group, subs, sends, rows_ref, place_ref, returned,
+    outgoing, tokens, parts, parts_in, sums, sums_in, final, w_gate, w_up, w_down,
+    zs, zr, ys, yr, cs, cr, ps, pr, qs, qr, bs, br, loads,
 ):
     grp = lax.axis_index("grp")
     me = lax.axis_index("ep")
     pairs = per_group // 2
     g, p = me // per_group, me % per_group
     q, c = p // 2, p % 2
-    depth = resid_ref.shape[1]
+    depth = returned.shape[2]
     cap = outgoing.shape[1]
     wide = outgoing.shape[2]
+    part = cap // subs
+    spans = [pl.ds(i * part, part) for i in range(subs)]
 
     def at(group, pair):
         return (grp, group * per_group + pair * 2 + c)
 
     mate = (grp, me + 1 - 2 * c)
-    others = [(g + i) % groups for i in range(1, groups)]
+    half = groups // 2
+    low = g // half * half
+    crossing = [(low + half) % groups + (g + i) % half for i in range(half)]
+    inside = [low + (g + i) % half for i in range(1, half)]
+    sources = [g] + inside + crossing
+    others = sources[1:]
     mates_q = [(q + j) % pairs for j in range(1, pairs)]
-    loads = [
-        pltpu.make_async_copy(gate_any.at[0], w_gate, w_sems.at[0]),
-        pltpu.make_async_copy(up_any.at[0], w_up, w_sems.at[1]),
-        pltpu.make_async_copy(down_any.at[0], w_down, w_sems.at[2]),
-    ]
-    for load in loads:
-        load.start()
     sent = lax.dot_general(place_ref[...], rows_ref[...], TN, preferred_element_type=F32).astype(BF16)
     outgoing[...] = sent.reshape(groups, cap, wide)
     tokens[g, c, q] = outgoing[g]
-    greet([at(o, q) for o in others] + [at(g, o) for o in mates_q] + [mate])
-    sends = []
 
     def start(copy):
         copy.start()
         sends.append(copy)
 
-    for target in others:
-        start(remote(outgoing.at[target], tokens.at[g, c, q], zs.at[target], zr.at[g], at(target, q)))
-
-    def source(i):
-        return (g + groups - i) % groups
-
-    def to_mate(s, pair):
-        spot = tokens.at[s, c, pair]
-        start(remote(spot, spot, cs.at[s, pair], cr.at[s, pair], mate))
-
-    def stage_a(i):
-        s = source(i)
-        spot = tokens.at[s, c, q]
-        if i > 0:
-            remote(spot, spot, zs.at[s], zr.at[s], mate).wait_recv()
+    for u in range(subs):
+        for target in others:
+            start(remote(
+                outgoing.at[target, spans[u]], tokens.at[g, c, q, spans[u]], zs.at[target, u], zr.at[g, u], at(target, q)
+            ))
+
+    def spread(k, u):
+        s = sources[k]
+        spot = tokens.at[s, c, q, spans[u]]
+        if k > 0:
+            remote(spot, spot, zs.at[s, u], zr.at[s, u], mate).wait_recv()
         for o in mates_q:
-            start(remote(spot, spot, ys.at[s, o], yr.at[s, q], at(g, o)))
-        to_mate(s, q)
-
-    def stage_b(i):
-        s = source(i)
+            start(remote(spot, spot, ys.at[s, o, u], yr.at[s, q, u], at(g, o)))
+        start(remote(spot, spot, cs.at[s, q, u], cr.at[s, q, u], mate))
+
+    def relay(k, u):
+        s = sources[k]
         for o in mates_q:
-            spot = tokens.at[s, c, o]
-            remote(spot, spot, ys.at[s, o], yr.at[s, o], mate).wait_recv()
-            to_mate(s, o)
-
-    def stage_c(i):
-        s = source(i)
+            spot = tokens.at[s, c, o, spans[u]]
+            remote(spot, spot, ys.at[s, o, u], yr.at[s, o, u], mate).wait_recv()
+            start(remote(spot, spot, cs.at[s, o, u], cr.at[s, o, u], mate))
+
+    def compute(k, u):
+        s = sources[k]
         for o in range(pairs):
-            spot = tokens.at[s, 1 - c, o]
-            remote(spot, spot, cs.at[s, o], cr.at[s, o], mate).wait_recv()
-        if i == 0:
+            spot = tokens.at[s, 1 - c, o, spans[u]]
+            remote(spot, spot, cs.at[s, o, u], cr.at[s, o, u], mate).wait_recv()
+        if k == 0 and u == 0:
             for load in loads:
                 load.wait()
-        total = per_group * cap
-        x = tokens[s].reshape(total, wide)
+        total = per_group * part
+        x = tokens[s, :, :, spans[u]].reshape(total, wide)
         rows = x[:, :depth]
         gate = jnp.dot(rows, w_gate[...], preferred_element_type=F32)
         upper = jnp.dot(rows, w_up[...], preferred_element_type=F32)
@@ -356,48 +343,128 @@
         lane = lax.broadcasted_iota(jnp.int32, (total, wide - depth), 1)
         mine = (lane == p) | (lane == p + per_group)
         weight = jnp.sum(jnp.where(mine, x[:, depth:].astype(F32), 0.0), axis=1, keepdims=True)
-        parts[s] = (result.astype(F32) * weight).astype(BF16).reshape(2, pairs, cap, depth)
-        start(remote(parts.at[s, 1 - c], parts_in.at[s], ps.at[s], pr.at[s], mate))
-
-    def stage_d(i):
-        s = source(i)
-        spot = parts_in.at[s]
-        remote(spot, spot, ps.at[s], pr.at[s], mate).wait_recv()
-        sums[s] = (parts[s, c].astype(F32) + parts_in[s].astype(F32)).astype(BF16)
+        parts[s, u] = (result.astype(F32) * weight).astype(BF16).reshape(2, pairs, part, depth)
+        start(remote(parts.at[s, u, 1 - c], parts_in.at[s, u], ps.at[s, u], pr.at[s, u], mate))
+
+    def reduce_mate(k, u):
+        s = sources[k]
+        spot = parts_in.at[s, u]
+        remote(spot, spot, ps.at[s, u], pr.at[s, u], mate).wait_recv()
+        sums[s, u] = (parts[s, u, c].astype(F32) + parts_in[s, u].astype(F32)).astype(BF16)
         for o in mates_q:
-            start(remote(sums.at[s, o], sums_in.at[s, q], qs.at[s, o], qr.at[s, q], at(g, o)))
-
-    def stage_e(i):
-        s = source(i)
-        total = sums[s, q].astype(F32)
+            start(remote(sums.at[s, u, o], sums_in.at[s, u, q], qs.at[s, o, u], qr.at[s, q, u], at(g, o)))
+
+    def reduce_pairs(k, u):
+        s = sources[k]
+        total = sums[s, u, q].astype(F32)
         for o in mates_q:
-            spot = sums_in.at[s, o]
-            remote(spot, spot, qs.at[s, o], qr.at[s, o], mate).wait_recv()
-            total = total + sums_in[s, o].astype(F32)
-        if i == 0:
-            returned[g] = total.astype(BF16)
+            spot = sums_in.at[s, u, o]
+            remote(spot, spot, qs.at[s, o, u], qr.at[s, o, u], mate).wait_recv()
+            total = total + sums_in[s, u, o].astype(F32)
+        if k == 0:
+            returned[g, spans[u]] = total.astype(BF16)
         else:
-            final[s] = total.astype(BF16)
-            start(remote(final.at[s], returned.at[g], bs.at[s], br.at[g], at(s, q)))
-
-    stage_a(0)
-    for t in range(groups):
-        stage_b(t)
-        if t + 1 < groups:
-            stage_a(t + 1)
-        stage_c(t)
-        stage_d(t)
-        if t > 0:
-            stage_e(t - 1)
-    stage_e(groups - 1)
+            final[s, spans[u]] = total.astype(BF16)
+            start(remote(
+                final.at[s, spans[u]], returned.at[g, spans[u]], bs.at[s, u], br.at[g, u], at(s, q)
+            ))
+
+    every = range(subs)
+    own, near, far = [0], list(range(1, half)), list(range(half, groups))
+    early, late = every[:1], every[1:]
+
+    def run(stage, kinds, units):
+        for u in units:
+            for k in kinds:
+                stage(k, u)
+
+    run(spread, own, every)
+    run(spread, near, early)
+    run(relay, own, every)
+    run(spread, far[:1], early)
+    run(compute, own, early)
+    run(spread, far[1:], early)
+    run(compute, own, late)
+    run(relay, near, early)
+    run(relay, far[:1], early)
+    run(compute, far[:1], early)
+    run(spread, near, late)
+    run(relay, far[1:], early)
+    run(compute, far[1:], early)
+    run(reduce_mate, far[:1], early)
+    run(spread, far[:1], late)
+    run(reduce_mate, far[1:], early)
+    run(spread, far[1:], late)
+    run(compute, near, early)
+    run(reduce_pairs, far, early)
+    run(reduce_mate, near, early)
+    run(relay, near, late)
+    run(relay, far[:1], late)
+    run(compute, far[:1], late)
+    run(relay, far[1:], late)
+    run(compute, far[1:], late)
+    run(reduce_mate, far, late)
+    run(compute, near, late)
+    run(reduce_pairs, far, late)
+    run(reduce_mate, near, late)
+    run(reduce_mate, own, every)
+    run(reduce_pairs, near, every)
+    run(reduce_pairs, own, every)
     for o in others:
-        spot = returned.at[o]
-        remote(spot, spot, bs.at[o], br.at[o], mate).wait_recv()
-    back = returned[...].reshape(groups * cap, depth)
+        for u in every:
+            spot = returned.at[o, spans[u]]
+            remote(spot, spot, bs.at[o, u], br.at[o, u], mate).wait_recv()
+
+
+def layer_kernel(
+    chips, groups, per_group, subs, *refs,
+):
+    inputs, outputs, scratch = refs[:21], refs[21:25], refs[25:]
+    weights = inputs[18:]
+    state, resid_ref, place_ref, returned = outputs
+    rows_ref, *rest = scratch
+    front_scratch, rest = rest[:12], rest[12:]
+    front_sems, rest = rest[:12], rest[12:]
+    expert_scratch, expert_sems = rest[:10], rest[10:]
+    loads = [
+        pltpu.make_async_copy(src.at[0], dst, expert_sems[-1].at[i])
+        for i, (src, dst) in enumerate(zip(weights, expert_scratch[7:]))
+    ]
+    sends = []
+
+    def meet(peers):
+        grp = lax.axis_index("grp")
+        me = lax.axis_index("ep")
+        g, p = me // per_group, me % per_group
+        ahead = [(grp, (g + i) % groups * per_group + p) for i in range(1, groups)]
+        near = [(grp, g * per_group + (p + 2 * i) % per_group) for i in range(1, per_group // 2)]
+        greet(peers + ahead + near)
+
+    front(
+        chips, per_group, sends, *inputs[:18], state, resid_ref, place_ref, rows_ref, *front_scratch, *front_sems,
+        meet, loads,
+    )
+    experts(
+        groups, per_group, subs, sends, rows_ref, place_ref, returned, *expert_scratch, *expert_sems[:-1], loads,
+    )
+    for copy in sends:
+        copy.wait_send()
+
+
+def finish_kernel(state_ref, resid_ref, place_ref, returned_ref, new_any, out_ref, sems):
+    copies = [
+        pltpu.make_async_copy(
+            state_ref.at[i, pl.ds(j * 64, 64)], new_any.at[i, pl.ds(j * 64, 64)], sems.at[i, j]
+        )
+        for i in range(2) for j in range(state_ref.shape[1] // 64)
+    ]
+    for copy in copies:
+        copy.start()
+    back = returned_ref[...].reshape(-1, returned_ref.shape[2])
     moe = jnp.dot(place_ref[...], back, preferred_element_type=F32)
     out_ref[...] = (resid_ref[...].astype(F32) + moe).astype(BF16)
-    for copy in sends:
-        copy.wait_send()
+    for copy in copies:
+        copy.wait()
 
 
 def on_device(
@@ -417,63 +484,61 @@
     experts = w_route.shape[1]
     per_group = experts // EXP_GROUPS
     cap = 2 * rows // EXP_GROUPS
-    new_state, resid, packed, place = pl.pallas_call(
-        functools.partial(front_kernel, chips, per_group),
-        out_shape=[
-            jax.ShapeDtypeStruct(state.shape, F32),
-            jax.ShapeDtypeStruct((rows, depth), BF16),
-            jax.ShapeDtypeStruct((rows, depth + 128), BF16),
-            jax.ShapeDtypeStruct((rows, EXP_GROUPS * cap), BF16),
-        ],
-        in_specs=[ANY, VMEM, ANY, ANY] + [VMEM] * 3 + [ANY] * 4 + [VMEM] * 2 + [ANY] * 2 + [VMEM] * 3,
-        out_specs=[ANY] + [VMEM] * 3,
+    pairs = per_group // 2
+    G = EXP_GROUPS
+    subs = cap // 32
+    part = cap // subs
+    vm = pltpu.VMEM
+    kept = [
+        vm(state.shape, F32), vm((rows, depth), BF16), vm((rows, G * cap), BF16), vm((G, cap, depth), BF16),
+    ]
+    results = pl.pallas_call(
+        functools.partial(layer_kernel, chips, G, per_group, subs),
+        out_shape=kept,
+        in_specs=[ANY, VMEM, ANY, ANY] + [VMEM] * 3 + [ANY] * 4 + [VMEM] * 2 + [ANY] * 2 + [VMEM] * 3 + [ANY] * 3,
+        out_specs=[VMEM] * 4,
         scratch_shapes=[
-            pltpu.VMEM((chips, 2, shard, depth), BF16),
-            pltpu.VMEM((rows, depth), BF16),
-            pltpu.VMEM(state.shape, F32),
-        ] + [pltpu.VMEM((channels, entries), F32)] * 4 + [
-            pltpu.VMEM(w_glu.shape, BF16),
-            pltpu.VMEM(w_out.shape, BF16),
-            pltpu.VMEM((rows, depth), BF16),
-            pltpu.VMEM((4, groups, entries), F32),
-            pltpu.VMEM((rows, channels), F32),
-            pltpu.VMEM((rows, channels), F32),
+            vm((rows, depth + 128), BF16),
+            vm((chips, 2, shard, depth), BF16),
+            vm((rows, depth), BF16),
+        ] + [vm((channels, entries), F32)] * 4 + [
+            vm(w_glu.shape, BF16),
+            vm(w_out.shape, BF16),
+            vm((rows, depth), BF16),
+            vm((4, groups, entries), F32),
+            vm((rows, channels), F32),
+            vm((rows, channels), F32),
         ] + [dma((lines, 2))] * 4 + [dma((chips,))] * 2 + [dma((chips, 3))] * 2
-        + [dma, dma, dma((8,)), dma((blocks,)), dma((blocks,))],
-        compiler_params=pltpu.CompilerParams(collective_id=0, has_side_effects=True, vmem_limit_bytes=FRONT_LIMIT),
-        name="front",
+        + [dma, dma, dma((8,)), dma((blocks,))] + [
+            vm((G, cap, depth + 128), BF16),
+            vm((G, 2, pairs, cap, depth + 128), BF16),
+            vm((G, subs, 2, pairs, part, depth), BF16),
+            vm((G, subs, pairs, part, depth), BF16),
+            vm((G, subs, pairs, part, depth), BF16),
+            vm((G, subs, pairs, part, depth), BF16),
+            vm((G, cap, depth), BF16),
+            vm(w_gate.shape[1:], BF16),
+            vm(w_up.shape[1:], BF16),
+            vm(w_down.shape[1:], BF16),
+        ] + [dma((G, subs))] * 2 + [dma((G, pairs, subs))] * 4 + [dma((G, subs))] * 2 + [dma((G, pairs, subs))] * 2
+        + [dma((G, subs))] * 2 + [dma((3,))],
+        compiler_params=pltpu.CompilerParams(collective_id=0, has_side_effects=True, vmem_limit_bytes=LIMIT),
+        name="layer",
     )(
         hidden, norm_gain[None, :], w_in.T, state, lam_re, lam_im, log_step[None, :],
         in_re.transpose(0, 2, 1).reshape(channels, entries), in_im.transpose(0, 2, 1).reshape(channels, entries),
         out_re.reshape(channels, entries), out_im.reshape(channels, entries), skip[None, :], ffn_gain[None, :],
-        w_glu, w_out, w_group.T, w_route.T, route_ids.T,
+        w_glu, w_out, w_group.T, w_route.T, route_ids.T, w_gate, w_up, w_down,
     )
-
-    pairs = per_group // 2
-    G = EXP_GROUPS
-    hidden_out = pl.pallas_call(
-        functools.partial(expert_kernel, G, per_group),
-        out_shape=jax.ShapeDtypeStruct((rows, depth), BF16),
-        in_specs=[VMEM] * 3 + [ANY] * 3,
-        out_specs=VMEM,
-        scratch_shapes=[
-            pltpu.VMEM((G, cap, depth + 128), BF16),
-            pltpu.VMEM((G, 2, pairs, cap, depth + 128), BF16),
-            pltpu.VMEM((G, 2, pairs, cap, depth), BF16),
-            pltpu.VMEM((G, pairs, cap, depth), BF16),
-            pltpu.VMEM((G, pairs, cap, depth), BF16),
-            pltpu.VMEM((G, pairs, cap, depth), BF16),
-            pltpu.VMEM((G, cap, depth), BF16),
-            pltpu.VMEM((G, cap, depth), BF16),
-            pltpu.VMEM(w_gate.shape[1:], BF16),
-            pltpu.VMEM(w_up.shape[1:], BF16),
-            pltpu.VMEM(w_down.shape[1:], BF16),
-            dma((G,)), dma((G,)), dma((G, pairs)), dma((G, pairs)), dma((G, pairs)), dma((G, pairs)),
-            dma((G,)), dma((G,)), dma((G, pairs)), dma((G, pairs)), dma((G,)), dma((G,)), dma((3,)),
-        ],
-        compiler_params=pltpu.CompilerParams(collective_id=1, has_side_effects=True, vmem_limit_bytes=LIMIT),
-        name="experts",
-    )(packed, place, resid, w_gate, w_up, w_down)
+    new_state, hidden_out = pl.pallas_call(
+        finish_kernel,
+        out_shape=[jax.ShapeDtypeStruct(state.shape, F32), jax.ShapeDtypeStruct((rows, depth), BF16)],
+        in_specs=[VMEM] * 4,
+        out_specs=[ANY, VMEM],
+        scratch_shapes=[dma((2, rows // 64))],
+        compiler_params=pltpu.CompilerParams(vmem_limit_bytes=FINISH_LIMIT),
+        name="finish",
+    )(*results)
     return (hidden_out, new_state)
 
 

time: 141 us -> 103 us (0.73)
  the two profiles are of different devices: /device:TPU:7 before, /device:TPU:0 now
where the time goes in v2:
time: 103 us
  Pallas kernels  102 us (99%)
    pallas_call x1, Pallas kernels, on_device(): pl.pallas_call(functools.partial(layer_kernel, chips, G, per_group, subs)...  99 us
    pallas_call x1, Pallas kernels, on_device(): pl.pallas_call(finish_kernel, out_shape=[jax.ShapeDtypeStruct(state.shape...  2.88 us

profile of v2, /device:TPU:0, one launch (start us, length us, event | category | flops | bytes accessed | tf_op | source)
XLA Modules:
  0.0 102.7 jit_solution(18100806056599695735)
XLA Ops:
  0.6 99.0 %layer.1 = (f32[2,128,4096]{2,1,0:T(8,128)S(1)}, bf16[128,2048]{1,0:T(8,128)(2,1)S(1)}, bf16[128,256]{1,0:T(8,128)(2,1)S(1)}, bf16[4,64,2048]{2,1,0:T(8,128)(2,1)S(1)}) custom-call(bf16[128,2048]{1,0:T(8,128)(2,1)} %refs_0_.1, f32[1,2048]{1,0:T(1,128)} %bitcast.23, bf16[64,2048]{1,0:T(8,128)(2,1)} %bitcast.20, f32[2,128,4096]{2,1,0:T(8,128)} %refs_3_.1, ...), custom_call_target="tpu_custom_call" | custom-call | tf_op jit(solution)/shard_map/layer/pallas_call | solution.py:495
  99.7 2.9 %finish.1 = (f32[2,128,4096]{2,1,0:T(8,128)}, bf16[128,2048]{1,0:T(8,128)(2,1)}) custom-call(f32[2,128,4096]{2,1,0:T(8,128)S(1)} %get-tuple-element.8.state_ref, bf16[128,2048]{1,0:T(8,128)(2,1)S(1)} %get-tuple-element.9.resid_ref, bf16[128,256]{1,0:T(8,128)(2,1)S(1)} %get-tuple-element.10.place_ref, bf16[4,64,2048]{2,1,0:T(8,128)(2,1)S(1)} %get-tuple-element.11.returned_ref), custom_call_target="tpu_custom_call" | custom-call | tf_op jit(solution)/shard_map/finish/pallas_call | solution.py:533

commit v3 on v2

--- a/solution.py
+++ b/solution.py
@@ -16,6 +16,19 @@
 BF16 = jnp.bfloat16
 NT = (((1,), (1,)), ((), ()))
 TN = (((0,), (0,)), ((), ()))
+GATHER_ORDER = (
+    "o0 a0 o1 a1", "b0 c0 b1 a2", "o2 a4 o5 A0", "o4 o3 A1 B0", "a3 a5 b2 om", "b4 c1 B1 b5",
+    "c4 b3 am c3", "A3 A4 A2 C0", "A5 bm c2 C1", "B4 c5 B2 B3", "B5 Am C4 Bm", "C3 C5 C2 cm",
+    "Cm",
+)
+SEND_ORDER = (
+    "20 10 30 21", "11 31 13 12", "22 23 32 33",
+)
+EXPERT_ORDER = (
+    "F00 F02 F01 G00", "F03 G02 G01 F20", "G03 F10 F30 C00", "F21 C01 G20 F11", "F31 F13 G30 G21", "G10 F12 C20 F22",
+    "G11 M20 G31 F23", "C10 M21 C30 E20", "G13 F32 G22 G12", "G23 M30 F33 E21", "C21 M31 M10 G32", "E30 C11 M22 G33",
+    "M11 M23 E31 C31", "E22 E10 M12 M32", "M33 E23 M00 M13", "M02 E11 E32 E12", "M03 M01 E33 E13", "E03 E02 E00 E01",
+)
 LIMIT = 57 * 1024 * 1024
 FINISH_LIMIT = 16 * 1024 * 1024
 
@@ -33,14 +46,8 @@
     pl.semaphore_wait(barrier, len(peers))
 
 
-def nearest(spot, count, k):
-    after = count - 1 - spot
-    longer = (after - spot + count - 1) // count
-    short = spot * longer + after * (1 - longer)
-    past = (k + 2 * count - 2 * short) // (2 * count)
-    paired = (k // 2 + 1) * (1 - 2 * (k % 2))
-    single = (k - short + 1) * (2 * longer - 1)
-    return spot + paired * (1 - past) + single * past
+def words(table):
+    return [word for text in table for word in text.split()]
 
 
 def front(
@@ -48,7 +55,7 @@
     out_re_any, out_im_any, skip_ref, ffn_gain_ref, w_glu_any, w_out_any, w_group_ref, w_route_ref, ids_ref,
     state, resid_ref, place_ref, rows_ref,
     held, hidden, in_re, in_im, out_re, out_im, glu_w, out_w, normed, coef, active, gating,
-    zs, zr, ys, yr, xs, xr, ds, dr, own_s, own_r, load_sems, state_sems, meet, expert_loads,
+    zs, zr, ys, yr, xs, xr, ds, dr, fs, own_s, own_r, load_sems, state_sems, meet, expert_loads,
 ):
     grp = lax.axis_index("grp")
     me = lax.axis_index("ep")
@@ -69,7 +76,17 @@
     mate = (grp, me + 1 - 2 * core)
     across = (grp + 1 - 2 * side, me)
     beside = at(line, 1 - y)
-    order = [nearest(line, lines, k) for k in range(lines - 1)]
+    half = lines // 2
+    high = line // half
+    low = high * half
+    inside = [low + (line + i) % half for i in range(1, half)]
+    crossing = [(half + i) * (1 - high) + (half - 1 - i) * high for i in range(half)]
+    order = inside + crossing
+    near_gate = (half - 1) * (1 - high) + half * high
+    far_gate = half * (1 - high) + (half - 1) * high
+    subs = 2
+    part = shard // subs
+    pieces = 2 * subs
     third = depth // 3 // 128 * 128
     middle = depth - 2 * third
     cols = [
@@ -82,8 +99,13 @@
         copy.start()
         sends.append(copy)
 
+    passed = []
+
+    def view(chip_at, core_at, p):
+        return held.at[chip_at, core_at, pl.ds(p % subs * part, part), cols[p // subs]]
+
     def column(j):
-        return pl.ds(pl.multiple_of(j * span, 128), span)
+        return pl.ds(pl.multiple_of(j * span, span), span)
 
     own = pltpu.make_async_copy(w_any, held.at[chip, core], load_sems.at[0])
     own.start()
@@ -98,10 +120,10 @@
         load.start()
     meet([at(o, y) for o in order] + [beside, mate, across])
     own.wait()
-    for p in range(2):
-        spot = held.at[chip, core, :, cols[p]]
+    for p in range(pieces):
+        spot = view(chip, core, p)
         start(remote(spot, spot, ys.at[line, p], yr.at[line, p], beside))
-        for o in order:
+        for o in inside + [far_gate]:
             start(remote(spot, spot, zs.at[o, p], zr.at[line, p], at(o, y)))
     spot = held.at[chip, core]
     start(remote(spot, spot, own_s, own_r, mate))
@@ -179,57 +201,76 @@
             return order[k] * 2 + y
         return (line if k < 0 else order[k]) * 2 + 1 - y
 
+    def forward(k, p, spot):
+        s = order[k]
+        copies = [
+            remote(spot, spot, fs.at[k - half + 1, p, i], zr.at[s, p], at(target, y)) for i, target in enumerate(inside)
+        ]
+        passed.extend(copies)
+
+        @pl.when(line == near_gate)
+        def _():
+            for copy in copies:
+                copy.start()
+
     def take(item, p):
         kind, k = item
         s = line if k < 0 else order[k]
-        spot = held.at[place(item), core, :, cols[p]]
+        spot = view(place(item), core, p)
         if kind == 0:
             remote(spot, spot, zs.at[s, p], zr.at[s, p], mate).wait_recv()
+            if k >= half - 1:
+                forward(k, p, spot)
             start(remote(spot, spot, ys.at[s, p], yr.at[s, p], beside))
         else:
             remote(spot, spot, ys.at[s, p], yr.at[s, p], mate).wait_recv()
-        if p == 0:
-            start(remote(spot, spot, xs.at[place(item)], xr.at[place(item)], across))
+        if p < subs:
+            start(remote(spot, spot, xs.at[place(item), p], xr.at[place(item), p], across))
         start(remote(spot, spot, ds.at[place(item), p], dr.at[place(item), p], mate))
 
-    def take_x(item):
-        spot = held.at[place(item), core, :, cols[2]]
-        remote(spot, spot, xs.at[place(item)], xr.at[place(item)], mate).wait_recv()
-        start(remote(spot, spot, ds.at[place(item), 2], dr.at[place(item), 2], mate))
-
-    def settle(item):
-        for p in range(3):
-            spot = held.at[place(item), 1 - core, :, cols[p]]
+    def take_x(item, u):
+        spot = view(place(item), core, pieces + u)
+        remote(spot, spot, xs.at[place(item), u], xr.at[place(item), u], mate).wait_recv()
+        start(remote(spot, spot, ds.at[place(item), pieces + u], dr.at[place(item), pieces + u], mate))
+
+    ready = {-1: 1}
+
+    def finish(item):
+        for p in range(pieces + subs):
+            spot = view(place(item), 1 - core, p)
             remote(spot, spot, ds.at[place(item), p], dr.at[place(item), p], mate).wait_recv()
-
-    items = [(1, -1)]
-    for k in range(lines):
-        if k < lines - 1:
-            items.append((0, k))
-        if k > 0:
-            items.append((1, k - 1))
+        if unit == 1:
+            mix(place(item))
+        else:
+            k = item[1]
+            ready[k] = ready.get(k, 0) + 1
+            if ready[k] == unit:
+                mix(line if k < 0 else order[k])
+
+    names = {"o": (1, -1), "a": (0, 0), "b": (0, 1), "c": (0, 2), "A": (1, 0), "B": (1, 1), "C": (1, 2)}
+    if lines == 4:
+        plan = [(names[word[0]], word[1]) for word in words(GATHER_ORDER)]
+    else:
+        items = [(1, -1)]
+        for k in range(lines):
+            if k < lines - 1:
+                items.append((0, k))
+            if k > 0:
+                items.append((1, k - 1))
+        plan = [(item, str(p)) for p in range(pieces) for item in items]
+        plan += [(item, step) for item in items for step in [str(pieces + u) for u in range(subs)] + ["m"]]
     spot = held.at[chip, 1 - core]
     remote(spot, spot, own_s, own_r, mate).wait_recv()
     loads[5].wait()
     if unit == 1:
         mix(chip)
-    for item in items:
-        take(item, 0)
-    ready = {-1: 1}
-    for at_ in range(len(items) + 1):
-        if at_ < len(items):
-            take(items[at_], 1)
-            if at_ == 0:
-                continue
-        take_x(items[at_ - 1])
-        settle(items[at_ - 1])
-        kind, k = items[at_ - 1]
-        if unit == 1:
-            mix(place(items[at_ - 1]))
+    for item, step in plan:
+        if step == "m":
+            finish(item)
+        elif int(step) < pieces:
+            take(item, int(step))
         else:
-            ready[k] = ready.get(k, 0) + 1
-            if ready[k] == unit:
-                mix(line if k < 0 else order[k])
+            take_x(item, int(step) - pieces)
     loads[6].wait()
 
     act = active[...]
@@ -267,9 +308,14 @@
     slot = group * (slots // EXP_GROUPS) + rank
     place_ref[...] = (iota((count, slots), 1) == slot).astype(BF16)
 
+    @pl.when(line == near_gate)
+    def _():
+        for copy in passed:
+            copy.wait_send()
+
 
 def experts(
-    groups, per_group, subs, sends, rows_ref, place_ref, returned,
+    groups, per_group, subs, chunks, sends, rows_ref, place_ref, returned,
     outgoing, tokens, parts, parts_in, sums, sums_in, final, w_gate, w_up, w_down,
     zs, zr, ys, yr, cs, cr, ps, pr, qs, qr, bs, br, loads,
 ):
@@ -303,11 +349,11 @@
         copy.start()
         sends.append(copy)
 
-    for u in range(subs):
-        for target in others:
-            start(remote(
-                outgoing.at[target, spans[u]], tokens.at[g, c, q, spans[u]], zs.at[target, u], zr.at[g, u], at(target, q)
-            ))
+    for word in words(SEND_ORDER):
+        target, u = sources[int(word[0])], int(word[1])
+        start(remote(
+            outgoing.at[target, spans[u]], tokens.at[g, c, q, spans[u]], zs.at[target, u], zr.at[g, u], at(target, q)
+        ))
 
     def spread(k, u):
         s = sources[k]
@@ -325,16 +371,24 @@
             remote(spot, spot, ys.at[s, o, u], yr.at[s, o, u], mate).wait_recv()
             start(remote(spot, spot, cs.at[s, o, u], cr.at[s, o, u], mate))
 
-    def compute(k, u):
+    fold = subs // chunks
+    bulk = cap // chunks
+
+    def inner_rows(u):
+        return pl.ds(u % fold * part, part)
+
+    def compute(k, h):
         s = sources[k]
-        for o in range(pairs):
-            spot = tokens.at[s, 1 - c, o, spans[u]]
-            remote(spot, spot, cs.at[s, o, u], cr.at[s, o, u], mate).wait_recv()
-        if k == 0 and u == 0:
+        for u in range(h * fold, h * fold + fold):
+            for o in range(pairs):
+                spot = tokens.at[s, 1 - c, o, spans[u]]
+                remote(spot, spot, cs.at[s, o, u], cr.at[s, o, u], mate).wait_recv()
+        if not loaded:
+            loaded.append(True)
             for load in loads:
                 load.wait()
-        total = per_group * part
-        x = tokens[s, :, :, spans[u]].reshape(total, wide)
+        total = per_group * bulk
+        x = tokens[s, :, :, pl.ds(h * bulk, bulk)].reshape(total, wide)
         rows = x[:, :depth]
         gate = jnp.dot(rows, w_gate[...], preferred_element_type=F32)
         upper = jnp.dot(rows, w_up[...], preferred_element_type=F32)
@@ -343,14 +397,21 @@
         lane = lax.broadcasted_iota(jnp.int32, (total, wide - depth), 1)
         mine = (lane == p) | (lane == p + per_group)
         weight = jnp.sum(jnp.where(mine, x[:, depth:].astype(F32), 0.0), axis=1, keepdims=True)
-        parts[s, u] = (result.astype(F32) * weight).astype(BF16).reshape(2, pairs, part, depth)
-        start(remote(parts.at[s, u, 1 - c], parts_in.at[s, u], ps.at[s, u], pr.at[s, u], mate))
+        parts[s, h] = (result.astype(F32) * weight).astype(BF16).reshape(2, pairs, bulk, depth)
+        start(remote(parts.at[s, h, 1 - c], parts_in.at[s, h], ps.at[s, h], pr.at[s, h], mate))
+
+    loaded = []
+    merged = set()
 
     def reduce_mate(k, u):
-        s = sources[k]
-        spot = parts_in.at[s, u]
-        remote(spot, spot, ps.at[s, u], pr.at[s, u], mate).wait_recv()
-        sums[s, u] = (parts[s, u, c].astype(F32) + parts_in[s, u].astype(F32)).astype(BF16)
+        s, h = sources[k], u // fold
+        if (k, h) not in merged:
+            merged.add((k, h))
+            spot = parts_in.at[s, h]
+            remote(spot, spot, ps.at[s, h], pr.at[s, h], mate).wait_recv()
+        sums[s, u] = (
+            parts[s, h, c, :, inner_rows(u)].astype(F32) + parts_in[s, h, :, inner_rows(u)].astype(F32)
+        ).astype(BF16)
         for o in mates_q:
             start(remote(sums.at[s, u, o], sums_in.at[s, u, q], qs.at[s, o, u], qr.at[s, q, u], at(g, o)))
 
@@ -369,62 +430,24 @@
                 final.at[s, spans[u]], returned.at[g, spans[u]], bs.at[s, u], br.at[g, u], at(s, q)
             ))
 
-    every = range(subs)
-    own, near, far = [0], list(range(1, half)), list(range(half, groups))
-    early, late = every[:1], every[1:]
-
-    def run(stage, kinds, units):
-        for u in units:
-            for k in kinds:
-                stage(k, u)
-
-    run(spread, own, every)
-    run(spread, near, early)
-    run(relay, own, every)
-    run(spread, far[:1], early)
-    run(compute, own, early)
-    run(spread, far[1:], early)
-    run(compute, own, late)
-    run(relay, near, early)
-    run(relay, far[:1], early)
-    run(compute, far[:1], early)
-    run(spread, near, late)
-    run(relay, far[1:], early)
-    run(compute, far[1:], early)
-    run(reduce_mate, far[:1], early)
-    run(spread, far[:1], late)
-    run(reduce_mate, far[1:], early)
-    run(spread, far[1:], late)
-    run(compute, near, early)
-    run(reduce_pairs, far, early)
-    run(reduce_mate, near, early)
-    run(relay, near, late)
-    run(relay, far[:1], late)
-    run(compute, far[:1], late)
-    run(relay, far[1:], late)
-    run(compute, far[1:], late)
-    run(reduce_mate, far, late)
-    run(compute, near, late)
-    run(reduce_pairs, far, late)
-    run(reduce_mate, near, late)
-    run(reduce_mate, own, every)
-    run(reduce_pairs, near, every)
-    run(reduce_pairs, own, every)
+    stages = {"F": spread, "G": relay, "C": compute, "M": reduce_mate, "E": reduce_pairs}
+    for word in words(EXPERT_ORDER):
+        stages[word[0]](int(word[1]), int(word[2]))
     for o in others:
-        for u in every:
+        for u in range(subs):
             spot = returned.at[o, spans[u]]
             remote(spot, spot, bs.at[o, u], br.at[o, u], mate).wait_recv()
 
 
 def layer_kernel(
-    chips, groups, per_group, subs, *refs,
+    chips, groups, per_group, subs, chunks, *refs,
 ):
     inputs, outputs, scratch = refs[:21], refs[21:25], refs[25:]
     weights = inputs[18:]
     state, resid_ref, place_ref, returned = outputs
     rows_ref, *rest = scratch
     front_scratch, rest = rest[:12], rest[12:]
-    front_sems, rest = rest[:12], rest[12:]
+    front_sems, rest = rest[:13], rest[13:]
     expert_scratch, expert_sems = rest[:10], rest[10:]
     loads = [
         pltpu.make_async_copy(src.at[0], dst, expert_sems[-1].at[i])
@@ -445,7 +468,7 @@
         meet, loads,
     )
     experts(
-        groups, per_group, subs, sends, rows_ref, place_ref, returned, *expert_scratch, *expert_sems[:-1], loads,
+        groups, per_group, subs, chunks, sends, rows_ref, place_ref, returned, *expert_scratch, *expert_sems[:-1], loads,
     )
     for copy in sends:
         copy.wait_send()
@@ -486,14 +509,14 @@
     cap = 2 * rows // EXP_GROUPS
     pairs = per_group // 2
     G = EXP_GROUPS
-    subs = cap // 32
-    part = cap // subs
+    subs, chunks = 4, 2
+    part, bulk = cap // subs, cap // chunks
     vm = pltpu.VMEM
     kept = [
         vm(state.shape, F32), vm((rows, depth), BF16), vm((rows, G * cap), BF16), vm((G, cap, depth), BF16),
     ]
     results = pl.pallas_call(
-        functools.partial(layer_kernel, chips, G, per_group, subs),
+        functools.partial(layer_kernel, chips, G, per_group, subs, chunks),
         out_shape=kept,
         in_specs=[ANY, VMEM, ANY, ANY] + [VMEM] * 3 + [ANY] * 4 + [VMEM] * 2 + [ANY] * 2 + [VMEM] * 3 + [ANY] * 3,
         out_specs=[VMEM] * 4,
@@ -508,19 +531,19 @@
             vm((4, groups, entries), F32),
             vm((rows, channels), F32),
             vm((rows, channels), F32),
-        ] + [dma((lines, 2))] * 4 + [dma((chips,))] * 2 + [dma((chips, 3))] * 2
-        + [dma, dma, dma((8,)), dma((blocks,))] + [
+        ] + [dma((lines, 4))] * 4 + [dma((chips, 2))] * 2 + [dma((chips, 6))] * 2
+        + [dma((lines // 2, 4, lines // 2 - 1)), dma, dma, dma((8,)), dma((blocks,))] + [
             vm((G, cap, depth + 128), BF16),
             vm((G, 2, pairs, cap, depth + 128), BF16),
-            vm((G, subs, 2, pairs, part, depth), BF16),
-            vm((G, subs, pairs, part, depth), BF16),
+            vm((G, chunks, 2, pairs, bulk, depth), BF16),
+            vm((G, chunks, pairs, bulk, depth), BF16),
             vm((G, subs, pairs, part, depth), BF16),
             vm((G, subs, pairs, part, depth), BF16),
             vm((G, cap, depth), BF16),
             vm(w_gate.shape[1:], BF16),
             vm(w_up.shape[1:], BF16),
             vm(w_down.shape[1:], BF16),
-        ] + [dma((G, subs))] * 2 + [dma((G, pairs, subs))] * 4 + [dma((G, subs))] * 2 + [dma((G, pairs, subs))] * 2
+        ] + [dma((G, subs))] * 2 + [dma((G, pairs, subs))] * 4 + [dma((G, chunks))] * 2 + [dma((G, pairs, subs))] * 2
         + [dma((G, subs))] * 2 + [dma((3,))],
         compiler_params=pltpu.CompilerParams(collective_id=0, has_side_effects=True, vmem_limit_bytes=LIMIT),
         name="layer",

time: 103 us -> 92.5 us (0.90)
  Pallas kernels: 102 us -> 91.5 us
    pallas_call x1, Pallas kernels: 99 us -> 88.6 us  [on_device(): pl.pallas_call(functools.partial(layer_kernel, chips, G, per_group, subs,...]
where the time goes in v3:
time: 92.5 us; the launch traced here: 92.3 us
  Pallas kernels  91.5 us (99%)
    pallas_call x1, Pallas kernels, on_device(): pl.pallas_call(functools.partial(layer_kernel, chips, G, per_group, subs,...  88.6 us
    pallas_call x1, Pallas kernels, on_device(): pl.pallas_call(finish_kernel, out_shape=[jax.ShapeDtypeStruct(state.shape...  2.88 us

profile of v3, /device:TPU:0, one launch (start us, length us, event | category | flops | bytes accessed | tf_op | source)
XLA Modules:
  0.0 92.3 jit_solution(116245804312617579)
XLA Ops:
  0.6 88.6 %layer.1 = (f32[2,128,4096]{2,1,0:T(8,128)S(1)}, bf16[128,2048]{1,0:T(8,128)(2,1)S(1)}, bf16[128,256]{1,0:T(8,128)(2,1)S(1)}, bf16[4,64,2048]{2,1,0:T(8,128)(2,1)S(1)}) custom-call(bf16[128,2048]{1,0:T(8,128)(2,1)} %refs_0_.1, f32[1,2048]{1,0:T(1,128)} %bitcast.23, bf16[64,2048]{1,0:T(8,128)(2,1)} %bitcast.20, f32[2,128,4096]{2,1,0:T(8,128)} %refs_3_.1, ...), custom_call_target="tpu_custom_call" | custom-call | tf_op jit(solution)/shard_map/layer/pallas_call | solution.py:518
  89.3 2.9 %finish.1 = (f32[2,128,4096]{2,1,0:T(8,128)}, bf16[128,2048]{1,0:T(8,128)(2,1)}) custom-call(f32[2,128,4096]{2,1,0:T(8,128)S(1)} %get-tuple-element.8.state_ref, bf16[128,2048]{1,0:T(8,128)(2,1)S(1)} %get-tuple-element.9.resid_ref, bf16[128,256]{1,0:T(8,128)(2,1)S(1)} %get-tuple-element.10.place_ref, bf16[4,64,2048]{2,1,0:T(8,128)(2,1)S(1)} %get-tuple-element.11.returned_ref), custom_call_target="tpu_custom_call" | custom-call | tf_op jit(solution)/shard_map/finish/pallas_call | solution.py:556

commit v4 on v3

v4 whole, which is shorter than its diff:
```python
import functools

import jax
import jax.numpy as jnp
from jax import lax
from jax.experimental import pallas as pl
from jax.experimental.pallas import tpu as pltpu
from jax.sharding import PartitionSpec as P

EXP_GROUPS = 4
TOPK = 2
MESH = pl.DeviceIdType.MESH
VMEM = pl.BlockSpec(memory_space=pltpu.VMEM)
ANY = pl.BlockSpec(memory_space=pl.ANY)
F32 = jnp.float32
BF16 = jnp.bfloat16
NT = (((1,), (1,)), ((), ()))
TN = (((0,), (0,)), ((), ()))
GATHER_ORDER = (
    "p o0 a0 w", "o1 a1 o2 b0", "c0 o4 b1 a4", "c1 A1 o3 o5", "a2 A0 a5 B0", "a3 b2 om c2",
    "am b3 B1 b4", "b5 C1 C0 A2", "c5 c4 c3 A5", "bm B2 A3 A4", "cm C2 B5 B4", "C5 B3 Am C4",
    "C3 Bm Cm",
)
SEND_ORDER = (
    "20 10 30 11", "21 13 31 12", "22 32 23 33",
)
EXPERT_ORDER = (
    "F00 F01 F02 F20", "G00 F03 G01 F10", "C00 F30 G03 G02", "F21 G20 F11 F13", "C01 G21 F31 F12", "G10 G30 C20 G11",
    "G13 F22 G31 M21", "M20 C30 F23 F32", "C10 E20 M30 E21", "G22 G23 M10 G12", "F33 M31 M11 C21", "G32 E30 C11 G33",
    "M22 M23 E31 E10", "M12 C31 E22 E11", "M02 M32 E23 M13", "M33 E12 E32 M01", "M03 E13 M00 E33", "E01 E03 E02 E00",
)
LIMIT = 57 * 1024 * 1024
FINISH_LIMIT = 16 * 1024 * 1024


def remote(src, dst, send_sem, recv_sem, device):
    return pltpu.make_async_remote_copy(
        src_ref=src, dst_ref=dst, send_sem=send_sem, recv_sem=recv_sem, device_id=device, device_id_type=MESH
    )


def greet(peers):
    barrier = pltpu.get_barrier_semaphore()
    for peer in peers:
        pl.semaphore_signal(barrier, inc=1, device_id=peer, device_id_type=MESH)
    pl.semaphore_wait(barrier, len(peers))


def words(table):
    return [word for text in table for word in text.split()]


def front(
    chips, per_group, sends, hidden_any, gain_any, w_any, state_any, lam_re_any, lam_im_any, step_any, in_re_any, in_im_any,
    out_re_any, out_im_any, skip_any, ffn_gain_any, w_glu_any, w_out_any, w_group_any, w_route_any, ids_any,
    state, resid_ref, place_ref, rows_ref, shares_ref, picks,
    held, hidden, in_re, in_im, out_re, out_im, glu_w, out_w, normed, coef, active, strips, into, outof, rounded,
    gain_ref, lam_re_ref, lam_im_ref, step_ref, skip_ref, ffn_gain_ref, w_group_ref, w_route_ref, ids_ref,
    zs, zr, ys, yr, xs, xr, ds, dr, fs, own_s, own_r, load_sems, state_sems, meet, expert_loads,
):
    grp = lax.axis_index("grp")
    me = lax.axis_index("ep")
    chip, core = me // 2, me % 2
    lines = chips // 2
    line, y = chip // 2, chip % 2
    side = grp % 2
    shard, depth = w_any.shape
    entries = lam_re_any.shape[1]
    unit = 128 // (2 * shard)
    blocks = chips // unit
    span = state.shape[2] // blocks
    channels = 128 // (span // entries)

    def at(row, column):
        return (grp, (row * 2 + column) * 2 + core)

    mate = (grp, me + 1 - 2 * core)
    across = (grp + 1 - 2 * side, me)
    beside = at(line, 1 - y)
    half = lines // 2
    high = line // half
    low = high * half
    inside = [low + (line + i) % half for i in range(1, half)]
    crossing = [(half + i) * (1 - high) + (half - 1 - i) * high for i in range(half)]
    order = inside + crossing
    near_gate = (half - 1) * (1 - high) + half * high
    far_gate = half * (1 - high) + (half - 1) * high
    subs = 2
    part = shard // subs
    pieces = 2 * subs
    third = depth // 3 // 128 * 128
    middle = depth - 2 * third
    cols = [
        pl.ds(pl.multiple_of(side * (depth - third), 128), third),
        pl.ds(third, middle),
        pl.ds(pl.multiple_of((1 - side) * (depth - third), 128), third),
    ]

    def start(copy):
        copy.start()
        sends.append(copy)

    passed = []

    def view(chip_at, core_at, p):
        return held.at[chip_at, core_at, pl.ds(p % subs * part, part), cols[p // subs]]

    def column(j):
        return pl.ds(pl.multiple_of(j * span, span), span)

    own = pltpu.make_async_copy(w_any, held.at[chip, core], load_sems.at[0])
    own.start()
    loads = [
        pltpu.make_async_copy(src, dst, load_sems.at[1 + i])
        for i, (src, dst) in enumerate([
            (hidden_any, hidden), (in_re_any, in_re), (in_im_any, in_im), (out_re_any, out_re), (out_im_any, out_im),
            (w_glu_any, glu_w), (w_out_any, out_w), (gain_any, gain_ref), (lam_re_any, lam_re_ref), (lam_im_any, lam_im_ref),
            (step_any, step_ref), (skip_any, skip_ref), (ffn_gain_any, ffn_gain_ref), (w_group_any, w_group_ref),
            (w_route_any, w_route_ref), (ids_any, ids_ref),
        ])
    ]
    block_loads = [
        pltpu.make_async_copy(state_any.at[:, :, pl.ds(j * span, span)], state.at[:, :, pl.ds(j * span, span)], state_sems.at[j])
        for j in range(blocks)
    ]
    for load in loads[:1] + loads[7:] + loads[1:5] + block_loads + loads[5:7] + expert_loads:
        load.start()
    meet([at(o, y) for o in order] + [beside, mate, across])
    own.wait()
    for p in range(pieces):
        spot = view(chip, core, p)
        start(remote(spot, spot, ys.at[line, p], yr.at[line, p], beside))
        for o in inside + [far_gate]:
            start(remote(spot, spot, zs.at[o, p], zr.at[line, p], at(o, y)))
    spot = held.at[chip, core]
    start(remote(spot, spot, own_s, own_r, mate))

    def iota(shape, axis):
        return lax.broadcasted_iota(jnp.int32, shape, axis)

    def prepare():
        for load in loads[:5] + loads[7:] + block_loads:
            load.wait()
        prepare_all()

    tiles = span // 128
    stack = tiles * blocks

    def twin(value):
        return jnp.concatenate([value] * (128 // entries), axis=1)

    def prepare_all():
        wide = hidden[...].astype(F32)
        mean = jnp.mean(wide * wide, axis=-1, keepdims=True)
        normed[...] = (wide * lax.rsqrt(mean + 1e-06) * gain_ref[...]).astype(BF16)

        groups = lam_re_ref.shape[0]
        lr, li = lam_re_ref[...], lam_im_ref[...]
        diagonal = iota((groups, groups), 0) == iota((groups, groups), 1)
        step = jnp.exp(jnp.sum(jnp.where(diagonal, step_ref[...], 0.0), axis=1, keepdims=True))
        magnitude = jnp.exp(lr * step)
        bar_re = magnitude * jnp.cos(li * step)
        bar_im = magnitude * jnp.sin(li * step)
        denom = lr * lr + li * li
        lessened = bar_re - 1.0
        first_half = iota((stack, 128), 1) < entries
        for i, value in enumerate([
            bar_re, bar_im, (lessened * lr + bar_im * li) / denom, (bar_im * lr - lessened * li) / denom,
        ]):
            coef[i] = twin(value)
            even, odd = coef[i, pl.ds(0, stack, stride=2), :], coef[i, pl.ds(1, stack, stride=2), :]
            chosen = jnp.where(first_half, even, odd)
            for j in range(blocks):
                strips[i, j] = chosen[j * tiles : (j + 1) * tiles]
        into[...] = jnp.zeros_like(into)
        outof[...] = jnp.zeros_like(outof)

        count = hidden.shape[0]
        lane = iota((count, 128), 1)
        same = (iota((count, count), 0) == iota((count, count), 1)).astype(BF16)
        ids = lax.dot_general(same, ids_ref[...].astype(F32).astype(BF16), NT, preferred_element_type=F32).astype(jnp.int32)
        group = ids[:, 0:1] // per_group
        hits = (lane == group).astype(BF16)
        earlier = (iota((count, count), 1) < iota((count, count), 0)).astype(BF16)
        before = jnp.dot(earlier, hits, preferred_element_type=F32)
        rank = jnp.sum(jnp.where(lane == group, before, 0.0), axis=1, keepdims=True).astype(jnp.int32)
        slots = place_ref.shape[1]
        slot = group * (slots // EXP_GROUPS) + rank
        place_ref[...] = (iota((count, slots), 1) == slot).astype(BF16)
        picks[...] = jnp.where(lane == 0, ids[:, 0:1], ids[:, 1:2])

    rise = 128 // tiles
    inside_tile = iota((128, 128), 0) // channels % 2 == iota((128, 128), 1) // entries

    def expand(ref, j, target, base, sign):
        part_of = ref[pl.ds(pl.multiple_of(j * 128, 128), 128), :]
        tile = jnp.where(inside_tile, twin(part_of), 0.0)
        tile = (tile if sign > 0 else -tile).astype(BF16)
        for t in range(tiles):
            target[t * rise : (t + 1) * rise, base + t * 128 : base + (t + 1) * 128] = tile[t * rise : (t + 1) * rise]

    def mix(j):
        expand(in_re, j, into, 0, 1)
        expand(in_im, j, into, span, 1)
        expand(out_re, j, outof, 0, 1)
        expand(out_im, j, outof, span, -1)
        block = held[pl.ds(j * unit, unit)].reshape(128, depth)
        inputs = lax.dot_general(normed[...], block, NT, preferred_element_type=F32).astype(BF16)
        drive = jnp.dot(inputs, into[...], preferred_element_type=F32)
        strip = [strips[i, j] for i in range(4)]
        for t in range(tiles):
            lanes = pl.ds(pl.multiple_of(j * span + t * 128, 128), 128)
            row = [value[t : t + 1] for value in strip]
            drive_re = drive[:, t * 128 : (t + 1) * 128]
            drive_im = drive[:, span + t * 128 : span + (t + 1) * 128]
            old_re, old_im = state[0, :, lanes], state[1, :, lanes]
            new_re = row[0] * old_re - row[1] * old_im + (row[2] * drive_re - row[3] * drive_im)
            new_im = row[0] * old_im + row[1] * old_re + (row[2] * drive_im + row[3] * drive_re)
            state[0, :, lanes] = new_re
            state[1, :, lanes] = new_im
            rounded[:, t * 128 : (t + 1) * 128] = new_re.astype(BF16)
            rounded[:, span + t * 128 : span + (t + 1) * 128] = new_im.astype(BF16)
        read = lax.dot_general(rounded[...], outof[...], NT, preferred_element_type=F32)
        lanes = pl.ds(pl.multiple_of(j * 128, 128), 128)
        act = jax.nn.gelu(read + skip_ref[:, lanes] * inputs.astype(F32))
        active[:, lanes] = act

    def place(item):
        kind, k = item
        if kind == 0:
            return order[k] * 2 + y
        return (line if k < 0 else order[k]) * 2 + 1 - y

    def forward(k, p, spot):
        s = order[k]
        copies = [
            remote(spot, spot, fs.at[k - half + 1, p, i], zr.at[s, p], at(target, y)) for i, target in enumerate(inside)
        ]
        passed.extend(copies)

        @pl.when(line == near_gate)
        def _():
            for copy in copies:
                copy.start()

    def take(item, p):
        kind, k = item
        s = line if k < 0 else order[k]
        spot = view(place(item), core, p)
        if kind == 0:
            remote(spot, spot, zs.at[s, p], zr.at[s, p], mate).wait_recv()
            if k >= half - 1:
                forward(k, p, spot)
            start(remote(spot, spot, ys.at[s, p], yr.at[s, p], beside))
        else:
            remote(spot, spot, ys.at[s, p], yr.at[s, p], mate).wait_recv()
        if p < subs:
            start(remote(spot, spot, xs.at[place(item), p], xr.at[place(item), p], across))
        start(remote(spot, spot, ds.at[place(item), p], dr.at[place(item), p], mate))

    def take_x(item, u):
        spot = view(place(item), core, pieces + u)
        remote(spot, spot, xs.at[place(item), u], xr.at[place(item), u], mate).wait_recv()
        start(remote(spot, spot, ds.at[place(item), pieces + u], dr.at[place(item), pieces + u], mate))

    ready = {-1: 1}

    def finish(item):
        for p in range(pieces + subs):
            spot = view(place(item), 1 - core, p)
            remote(spot, spot, ds.at[place(item), p], dr.at[place(item), p], mate).wait_recv()
        if unit == 1:
            mix(place(item))
        else:
            k = item[1]
            ready[k] = ready.get(k, 0) + 1
            if ready[k] == unit:
                mix(line if k < 0 else order[k])

    names = {"o": (1, -1), "a": (0, 0), "b": (0, 1), "c": (0, 2), "A": (1, 0), "B": (1, 1), "C": (1, 2)}
    if lines == 4:
        plan = [(names.get(word[0]), word[-1]) for word in words(GATHER_ORDER)]
    else:
        items = [(1, -1)]
        for k in range(lines):
            if k < lines - 1:
                items.append((0, k))
            if k > 0:
                items.append((1, k - 1))
        plan = [(None, "p"), (None, "w")] + [(item, str(p)) for p in range(pieces) for item in items]
        plan += [(item, step) for item in items for step in [str(pieces + u) for u in range(subs)] + ["m"]]
    for item, step in plan:
        if step == "p":
            prepare()
        elif step == "w":
            spot = held.at[chip, 1 - core]
            remote(spot, spot, own_s, own_r, mate).wait_recv()
            if unit == 1:
                mix(chip)
        elif step == "m":
            finish(item)
        elif int(step) < pieces:
            take(item, int(step))
        else:
            take_x(item, int(step) - pieces)
    loads[5].wait()
    loads[6].wait()

    act = active[...]
    gating = jnp.dot(act.astype(BF16), glu_w[...], preferred_element_type=F32)
    glu = (act * jax.nn.sigmoid(gating)).astype(BF16)
    resid = (hidden[...].astype(F32) + jnp.dot(glu, out_w[...], preferred_element_type=F32)).astype(BF16)
    resid_ref[...] = resid
    wide = resid.astype(F32)
    mean = jnp.mean(wide * wide, axis=-1, keepdims=True)
    second_normed = (wide * lax.rsqrt(mean + 1e-06) * ffn_gain_ref[...]).astype(BF16)
    rows_ref[...] = second_normed

    def share_out():
        level = lax.dot_general(rows_ref[...], w_group_ref[...], NT, preferred_element_type=F32)
        logits = lax.dot_general(rows_ref[...], w_route_ref[...], NT, preferred_element_type=F32)
        first, second = picks[:, 0:1], picks[:, 1:2]
        lane = iota(picks.shape, 1)
        group = first // per_group
        chosen = jnp.sum(jnp.where(iota(level.shape, 1) == group, level, 0.0), axis=1, keepdims=True)
        scale = 1.0 / jnp.sum(jnp.exp(level - chosen), axis=1, keepdims=True)
        r0 = jnp.sum(jnp.where(iota(logits.shape, 1) == first, logits, 0.0), axis=1, keepdims=True)
        r1 = jnp.sum(jnp.where(iota(logits.shape, 1) == second, logits, 0.0), axis=1, keepdims=True)
        share = jax.nn.sigmoid(r0 - r1)
        member = lane % per_group
        gate = jnp.where(member == first % per_group, scale * share, 0.0)
        gate = gate + jnp.where(member == second % per_group, scale * (1.0 - share), 0.0)
        high = gate.astype(BF16).astype(F32)
        low_lanes = (lane >= 8) & (lane < 8 + per_group)
        shares_ref[...] = jnp.where(lane < per_group, high, jnp.where(low_lanes, gate - high, 0.0)).astype(BF16)
        return lax.dot_general(shares_ref[...], place_ref[...], TN, preferred_element_type=F32)

    @pl.when(line == near_gate)
    def _():
        for copy in passed:
            copy.wait_send()
    return share_out


def experts(
    groups, per_group, subs, chunks, sends, rows_ref, shares_ref, place_ref, returned,
    outgoing, tokens, parts, parts_in, sums, sums_in, final, w_gate, w_up, w_down, shares, shares_in,
    zs, zr, ys, yr, cs, cr, ps, pr, qs, qr, bs, br, gs, gr, hs, hr, ks, kr, loads, share_out,
):
    grp = lax.axis_index("grp")
    me = lax.axis_index("ep")
    pairs = per_group // 2
    g, p = me // per_group, me % per_group
    q, c = p // 2, p % 2
    depth = returned.shape[2]
    cap = outgoing.shape[1]
    wide = outgoing.shape[2]
    part = cap // subs
    spans = [pl.ds(i * part, part) for i in range(subs)]

    def at(group, pair):
        return (grp, group * per_group + pair * 2 + c)

    mate = (grp, me + 1 - 2 * c)
    half = groups // 2
    low = g // half * half
    crossing = [(low + half) % groups + (g + i) % half for i in range(half)]
    inside = [low + (g + i) % half for i in range(1, half)]
    sources = [g] + inside + crossing
    others = sources[1:]
    mates_q = [(q + j) % pairs for j in range(1, pairs)]
    sent = lax.dot_general(place_ref[...], rows_ref[...], TN, preferred_element_type=F32).astype(BF16)
    outgoing[...] = sent.reshape(groups, cap, wide)
    tokens[g, c, q] = outgoing[g]
    per_tile = 128 // cap

    def start(copy):
        copy.start()
        sends.append(copy)


    def share():
        split = share_out()
        joined = split[0:8] + split[8:16]
        for i in range(groups // per_tile):
            shares[i] = joined[:, i * 128 : (i + 1) * 128]
        shares_in[g, c, q] = shares[g // per_tile]
        for target in others:
            start(remote(shares.at[target // per_tile], shares_in.at[g, c, q], gs.at[target], gr.at[g], at(target, q)))
        pass_shares(0)

    def pass_shares(k):
        s = sources[k]
        spot = shares_in.at[s, c, q]
        if k > 0:
            remote(spot, spot, gs.at[s], gr.at[s], mate).wait_recv()
        for o in mates_q:
            start(remote(spot, spot, hs.at[s, o], hr.at[s, q], at(g, o)))
        start(remote(spot, spot, ks.at[s, q], kr.at[s, q], mate))

    def dispatch(plan):
        for word in plan:
            target, u = sources[int(word[0])], int(word[1])
            start(remote(
                outgoing.at[target, spans[u]], tokens.at[g, c, q, spans[u]], zs.at[target, u], zr.at[g, u], at(target, q)
            ))

    started = {"F": set(), "G": set(), "C": set()}

    def first_of(stage, k):
        fresh = k not in started[stage]
        started[stage].add(k)
        return fresh

    def spread(k, u):
        s = sources[k]
        if first_of("F", k) and k > 0:
            pass_shares(k)
        spot = tokens.at[s, c, q, spans[u]]
        if k > 0:
            remote(spot, spot, zs.at[s, u], zr.at[s, u], mate).wait_recv()
        for o in mates_q:
            start(remote(spot, spot, ys.at[s, o, u], yr.at[s, q, u], at(g, o)))
        start(remote(spot, spot, cs.at[s, q, u], cr.at[s, q, u], mate))

    def relay(k, u):
        s = sources[k]
        if first_of("G", k):
            for o in mates_q:
                spot = shares_in.at[s, c, o]
                remote(spot, spot, hs.at[s, o], hr.at[s, o], mate).wait_recv()
                start(remote(spot, spot, ks.at[s, o], kr.at[s, o], mate))
        for o in mates_q:
            spot = tokens.at[s, c, o, spans[u]]
            remote(spot, spot, ys.at[s, o, u], yr.at[s, o, u], mate).wait_recv()
            start(remote(spot, spot, cs.at[s, o, u], cr.at[s, o, u], mate))

    fold = subs // chunks
    bulk = cap // chunks

    def inner_rows(u):
        return pl.ds(u % fold * part, part)

    spread_rows = lax.broadcasted_iota(jnp.int32, (bulk, 128), 0)
    spread_lanes = lax.broadcasted_iota(jnp.int32, (bulk, 128), 1)

    def compute(k, h):
        s = sources[k]
        if first_of("C", k):
            for o in range(pairs):
                spot = shares_in.at[s, 1 - c, o]
                remote(spot, spot, ks.at[s, o], kr.at[s, o], mate).wait_recv()
        for u in range(h * fold, h * fold + fold):
            for o in range(pairs):
                spot = tokens.at[s, 1 - c, o, spans[u]]
                remote(spot, spot, cs.at[s, o, u], cr.at[s, o, u], mate).wait_recv()
        if not loaded:
            loaded.append(True)
            for load in loads:
                load.wait()
        total = per_group * bulk
        x = tokens[s, :, :, pl.ds(h * bulk, bulk)].reshape(total, wide)
        gate = jnp.dot(x, w_gate[...], preferred_element_type=F32)
        upper = jnp.dot(x, w_up[...], preferred_element_type=F32)
        inner = (jax.nn.silu(gate) * upper).astype(BF16)
        result = jnp.dot(inner, w_down[...], preferred_element_type=F32).astype(BF16)
        own_lane = spread_lanes == spread_rows + (g % per_tile * cap + h * bulk)
        weight = jnp.concatenate([
            jnp.sum(jnp.where(own_lane, shares_in[s, i, o, pl.ds(p, 1), :], 0.0), axis=1, keepdims=True)
            for i in range(2) for o in range(pairs)
        ], axis=0)
        parts[s, h] = (result.astype(F32) * weight).astype(BF16).reshape(2, pairs, bulk, depth)
        start(remote(parts.at[s, h, 1 - c], parts_in.at[s, h], ps.at[s, h], pr.at[s, h], mate))

    loaded = []
    merged = set()

    def reduce_mate(k, u):
        s, h = sources[k], u // fold
        if (k, h) not in merged:
            merged.add((k, h))
            spot = parts_in.at[s, h]
            remote(spot, spot, ps.at[s, h], pr.at[s, h], mate).wait_recv()
        sums[s, u] = (
            parts[s, h, c, :, inner_rows(u)].astype(F32) + parts_in[s, h, :, inner_rows(u)].astype(F32)
        ).astype(BF16)
        for o in mates_q:
            start(remote(sums.at[s, u, o], sums_in.at[s, u, q], qs.at[s, o, u], qr.at[s, q, u], at(g, o)))

    def reduce_pairs(k, u):
        s = sources[k]
        total = sums[s, u, q].astype(F32)
        for o in mates_q:
            spot = sums_in.at[s, u, o]
            remote(spot, spot, qs.at[s, o, u], qr.at[s, o, u], mate).wait_recv()
            total = total + sums_in[s, u, o].astype(F32)
        if k == 0:
            returned[g, spans[u]] = total.astype(BF16)
        else:
            final[s, spans[u]] = total.astype(BF16)
            start(remote(
                final.at[s, spans[u]], returned.at[g, spans[u]], bs.at[s, u], br.at[g, u], at(s, q)
            ))

    stages = {"F": spread, "G": relay, "C": compute, "M": reduce_mate, "E": reduce_pairs}
    plan = words(EXPERT_ORDER)
    lead = [word[:2] == "F0" for word in plan + [""]].index(False)
    dispatch(words(SEND_ORDER)[:3])
    for word in plan[:lead]:
        spread(0, int(word[2]))
    share()
    dispatch(words(SEND_ORDER)[3:])
    for word in plan[lead:]:
        stages[word[0]](int(word[1]), int(word[2]))
    for o in others:
        for u in range(subs):
            spot = returned.at[o, spans[u]]
            remote(spot, spot, bs.at[o, u], br.at[o, u], mate).wait_recv()


def layer_kernel(
    chips, groups, per_group, subs, chunks, *refs,
):
    inputs, outputs, scratch = refs[:21], refs[21:25], refs[25:]
    weights = inputs[18:]
    state, resid_ref, place_ref, returned = outputs
    rows_ref, shares_ref, picks, *rest = scratch
    front_scratch, rest = rest[:24], rest[24:]
    front_sems, rest = rest[:13], rest[13:]
    expert_scratch, expert_sems = rest[:12], rest[12:]
    loads = [
        pltpu.make_async_copy(src.at[0], dst, expert_sems[-1].at[i])
        for i, (src, dst) in enumerate(zip(weights, expert_scratch[7:10]))
    ]
    sends = []

    def meet(peers):
        grp = lax.axis_index("grp")
        me = lax.axis_index("ep")
        g, p = me // per_group, me % per_group
        ahead = [(grp, (g + i) % groups * per_group + p) for i in range(1, groups)]
        near = [(grp, g * per_group + (p + 2 * i) % per_group) for i in range(1, per_group // 2)]
        greet(peers + ahead + near)

    share_out = front(
        chips, per_group, sends, *inputs[:18], state, resid_ref, place_ref, rows_ref, shares_ref, picks,
        *front_scratch, *front_sems,
        meet, loads,
    )
    experts(
        groups, per_group, subs, chunks, sends, rows_ref, shares_ref, place_ref, returned,
        *expert_scratch, *expert_sems[:-1], loads,
        share_out,
    )
    for copy in sends:
        copy.wait_send()


def finish_kernel(state_ref, resid_ref, place_ref, returned_ref, new_any, out_any, out, sems, out_sem):
    count = sems.shape[1]
    step = state_ref.shape[1] // count
    copies = [
        pltpu.make_async_copy(
            state_ref.at[i, pl.ds(j * step, step)], new_any.at[i, pl.ds(j * step, step)], sems.at[i, j]
        )
        for i in range(2) for j in range(count)
    ]
    for copy in copies:
        copy.start()
    back = returned_ref[...].reshape(-1, returned_ref.shape[2])
    moe = jnp.dot(place_ref[...], back, preferred_element_type=F32)
    out[...] = (resid_ref[...].astype(F32) + moe).astype(BF16)
    copies.append(pltpu.make_async_copy(out, out_any, out_sem))
    copies[-1].start()
    for copy in copies:
        copy.wait()


def on_device(
    hidden, state, norm_gain, w_in, lam_re, lam_im, log_step, in_re, in_im, out_re, out_im, skip, w_glu, w_out,
    ffn_gain, w_group, w_route, w_gate, w_up, w_down, route_ids,
):
    rows, depth = hidden.shape
    devices = lax.axis_size("ep")
    chips = devices // 2
    shard = w_in.shape[1]
    dma = pltpu.SemaphoreType.DMA
    groups, entries = lam_re.shape
    width = in_re.shape[2]
    channels = groups * width
    lines = chips // 2
    blocks = channels // 128
    experts = w_route.shape[1]
    per_group = experts // EXP_GROUPS
    cap = 2 * rows // EXP_GROUPS
    pairs = per_group // 2
    G = EXP_GROUPS
    subs, chunks = 4, 2
    part, bulk = cap // subs, cap // chunks
    vm = pltpu.VMEM
    kept = [
        vm(state.shape, F32), vm((rows, depth), BF16), vm((rows, G * cap), BF16), vm((G, cap, depth), BF16),
    ]
    results = pl.pallas_call(
        functools.partial(layer_kernel, chips, G, per_group, subs, chunks),
        out_shape=kept,
        in_specs=[ANY] * 21,
        out_specs=[VMEM] * 4,
        scratch_shapes=[
            vm((rows, depth), BF16),
            vm((rows, 128), BF16),
            vm((rows, 128), jnp.int32),
            vm((chips, 2, shard, depth), BF16),
            vm((rows, depth), BF16),
        ] + [vm((channels, entries), F32)] * 4 + [
            vm(w_glu.shape, BF16),
            vm(w_out.shape, BF16),
            vm((rows, depth), BF16),
            vm((4, groups, 128), F32),
            vm((rows, channels), F32),
            vm((4, blocks, groups * entries // blocks // 128, 128), F32),
            vm((128, 2 * groups * entries // blocks), BF16),
            vm((128, 2 * groups * entries // blocks), BF16),
            vm((rows, 2 * groups * entries // blocks), BF16),
            vm((1, depth), F32), vm((groups, entries), F32), vm((groups, entries), F32), vm((1, groups), F32),
            vm((1, channels), F32), vm((1, depth), F32), vm((EXP_GROUPS, depth), BF16), vm((experts, depth), BF16),
            vm((TOPK, rows), jnp.int32),
        ] + [dma((lines, 4))] * 4 + [dma((chips, 2))] * 2 + [dma((chips, 6))] * 2
        + [dma((lines // 2, 4, lines // 2 - 1)), dma, dma, dma((17,)), dma((blocks,))] + [
            vm((G, cap, depth), BF16),
            vm((G, 2, pairs, cap, depth), BF16),
            vm((G, chunks, 2, pairs, bulk, depth), BF16),
            vm((G, chunks, pairs, bulk, depth), BF16),
            vm((G, subs, pairs, part, depth), BF16),
            vm((G, subs, pairs, part, depth), BF16),
            vm((G, cap, depth), BF16),
            vm(w_gate.shape[1:], BF16),
            vm(w_up.shape[1:], BF16),
            vm(w_down.shape[1:], BF16),
            vm((G * cap // 128, 8, 128), F32),
            vm((G, 2, pairs, 8, 128), F32),
        ] + [dma((G, subs))] * 2 + [dma((G, pairs, subs))] * 4 + [dma((G, chunks))] * 2 + [dma((G, pairs, subs))] * 2
        + [dma((G, subs))] * 2 + [dma((G,))] * 2 + [dma((G, pairs))] * 4 + [dma((3,))],
        compiler_params=pltpu.CompilerParams(collective_id=0, has_side_effects=True, vmem_limit_bytes=LIMIT),
        name="layer",
    )(
        hidden, norm_gain[None, :], w_in.T, state, lam_re, lam_im, log_step[None, :],
        in_re.transpose(0, 2, 1).reshape(channels, entries), in_im.transpose(0, 2, 1).reshape(channels, entries),
        out_re.reshape(channels, entries), out_im.reshape(channels, entries), skip[None, :], ffn_gain[None, :],
        w_glu, w_out, w_group.T, w_route.T, route_ids.T, w_gate, w_up, w_down,
    )
    new_state, hidden_out = pl.pallas_call(
        finish_kernel,
        out_shape=[jax.ShapeDtypeStruct(state.shape, F32), jax.ShapeDtypeStruct((rows, depth), BF16)],
        in_specs=[VMEM] * 4,
        out_specs=[ANY, ANY],
        scratch_shapes=[vm((rows, depth), BF16), dma((2, rows // 16)), dma],
        compiler_params=pltpu.CompilerParams(vmem_limit_bytes=FINISH_LIMIT),
        name="finish",
    )(*results)
    return (hidden_out, new_state)


def solution(mesh):
    return jax.shard_map(
        on_device,
        mesh=mesh,
        in_specs=(
            P(("grp", "ep"), None),
            P(None, ("grp", "ep"), None),
            P(),
            P(None, "ep"),
            P(),
            P(),
            P(),
            P(),
            P(),
            P(),
            P(),
            P(),
            P(),
            P(),
            P(),
            P(),
            P(),
            P("ep", None, None),
            P("ep", None, None),
            P("ep", None, None),
            P(("grp", "ep"), None),
        ),
        out_specs=(P(("grp", "ep"), None), P(None, ("grp", "ep"), None)),
        check_vma=False,
    )
```

time: 92.5 us -> 86.3 us (0.933)
  Pallas kernels: 91.5 us -> 85.3 us
    pallas_call x1, Pallas kernels: 88.6 us -> 83 us  [on_device(): pl.pallas_call(functools.partial(layer_kernel, chips, G, per_group, subs,...]
where the time goes in v4:
time: 86.3 us; the launch traced here: 86.1 us
  Pallas kernels  85.3 us (99%)
    pallas_call x1, Pallas kernels, on_device(): pl.pallas_call(functools.partial(layer_kernel, chips, G, per_group, subs,...  83 us
    pallas_call x1, Pallas kernels, on_device(): pl.pallas_call(finish_kernel, out_shape=[jax.ShapeDtypeStruct(state.shape...  2.32 us

profile of v4, /device:TPU:0, one launch (start us, length us, event | category | flops | bytes accessed | tf_op | source)
XLA Modules:
  0.0 86.1 jit_solution(797635462754144507)
XLA Ops:
  0.6 83.0 %layer.1 = (f32[2,128,4096]{2,1,0:T(8,128)S(1)}, bf16[128,2048]{1,0:T(8,128)(2,1)S(1)}, bf16[128,256]{1,0:T(8,128)(2,1)S(1)}, bf16[4,64,2048]{2,1,0:T(8,128)(2,1)S(1)}) custom-call(bf16[128,2048]{1,0:T(8,128)(2,1)} %refs_0_.1, f32[1,2048]{1,0:T(1,128)} %bitcast.23, bf16[64,2048]{1,0:T(8,128)(2,1)} %bitcast.20, f32[2,128,4096]{2,1,0:T(8,128)} %refs_3_.1, ...), custom_call_target="tpu_custom_call" | custom-call | tf_op jit(solution)/shard_map/layer/pallas_call | solution.py:604
  83.6 2.3 %finish.1 = (f32[2,128,4096]{2,1,0:T(8,128)}, bf16[128,2048]{1,0:T(8,128)(2,1)}) custom-call(f32[2,128,4096]{2,1,0:T(8,128)S(1)} %get-tuple-element.8.state_ref, bf16[128,2048]{1,0:T(8,128)(2,1)S(1)} %get-tuple-element.9.resid_ref, bf16[128,256]{1,0:T(8,128)(2,1)S(1)} %get-tuple-element.10.place_ref, bf16[4,64,2048]{2,1,0:T(8,128)(2,1)S(1)} %get-tuple-element.11.returned_ref), custom_call_target="tpu_custom_call" | custom-call | tf_op jit(solution)/shard_map/finish/pallas_call | solution.py:652

commit v5 on v4

--- a/solution.py
+++ b/solution.py
@@ -17,17 +17,17 @@
 NT = (((1,), (1,)), ((), ()))
 TN = (((0,), (0,)), ((), ()))
 GATHER_ORDER = (
-    "p o0 a0 w", "o1 a1 o2 b0", "c0 o4 b1 a4", "c1 A1 o3 o5", "a2 A0 a5 B0", "a3 b2 om c2",
-    "am b3 B1 b4", "b5 C1 C0 A2", "c5 c4 c3 A5", "bm B2 A3 A4", "cm C2 B5 B4", "C5 B3 Am C4",
-    "C3 Bm Cm",
+    "p o0 a0 w", "o1 a1 b0 c0", "o4 o2 c1 b1", "A0 o5 a4 a2", "c2 a3 a5 o3", "A1 B0 b4 b2",
+    "C0 am c3 C1", "c4 c5 om b5", "B1 b3 A2 cm", "A4 A3 A5 bm", "B4 C2 C4 B2", "C5 C3 Am B3",
+    "B5 Cm Bm",
 )
 SEND_ORDER = (
-    "20 10 30 11", "21 13 31 12", "22 32 23 33",
+    "30 11 20 10", "21 12 31 13", "22 32 23 33",
 )
 EXPERT_ORDER = (
-    "F00 F01 F02 F20", "G00 F03 G01 F10", "C00 F30 G03 G02", "F21 G20 F11 F13", "C01 G21 F31 F12", "G10 G30 C20 G11",
-    "G13 F22 G31 M21", "M20 C30 F23 F32", "C10 E20 M30 E21", "G22 G23 M10 G12", "F33 M31 M11 C21", "G32 E30 C11 G33",
-    "M22 M23 E31 E10", "M12 C31 E22 E11", "M02 M32 E23 M13", "M33 E12 E32 M01", "M03 E13 M00 E33", "E01 E03 E02 E00",
+    "F00 F02 F01 F03", "F11 G01 G00 F20", "G03 G02 F10 C00", "F21 F30 G20 C01", "F12 F31 G21 F13", "C20 F22 G30 G31",
+    "G10 M20 M21 C30", "G11 F23 E20 G22", "F32 M31 C10 G23", "F33 M30 E21 C21", "M11 E31 G33 G32", "G13 M22 M10 E30",
+    "C31 M23 M03 G12", "E11 E22 M33 C11", "M32 E23 E10 M12", "M13 M00 E33 M01", "E12 E32 M02 E13", "E02 E00 E01 E03",
 )
 LIMIT = 57 * 1024 * 1024
 FINISH_LIMIT = 16 * 1024 * 1024
@@ -505,11 +505,11 @@
     stages = {"F": spread, "G": relay, "C": compute, "M": reduce_mate, "E": reduce_pairs}
     plan = words(EXPERT_ORDER)
     lead = [word[:2] == "F0" for word in plan + [""]].index(False)
-    dispatch(words(SEND_ORDER)[:3])
+    dispatch(words(SEND_ORDER)[:1])
     for word in plan[:lead]:
         spread(0, int(word[2]))
     share()
-    dispatch(words(SEND_ORDER)[3:])
+    dispatch(words(SEND_ORDER)[1:])
     for word in plan[lead:]:
         stages[word[0]](int(word[1]), int(word[2]))
     for o in others:

time: 86.3 us -> 85.6 us (level)
  no operation moved by 1% of the time
where the time goes in v5:
time: 85.6 us; the launch traced here: 85.5 us
  Pallas kernels  84.7 us (99%)
    pallas_call x1, Pallas kernels, on_device(): pl.pallas_call(functools.partial(layer_kernel, chips, G, per_group, subs,...  82.4 us
    pallas_call x1, Pallas kernels, on_device(): pl.pallas_call(finish_kernel, out_shape=[jax.ShapeDtypeStruct(state.shape...  2.32 us

profile of v5, /device:TPU:0, one launch (start us, length us, event | category | flops | bytes accessed | tf_op | source)
XLA Modules:
  0.0 85.5 jit_solution(16206778317507566912)
XLA Ops:
  0.6 82.4 %layer.1 = (f32[2,128,4096]{2,1,0:T(8,128)S(1)}, bf16[128,2048]{1,0:T(8,128)(2,1)S(1)}, bf16[128,256]{1,0:T(8,128)(2,1)S(1)}, bf16[4,64,2048]{2,1,0:T(8,128)(2,1)S(1)}) custom-call(bf16[128,2048]{1,0:T(8,128)(2,1)} %refs_0_.1, f32[1,2048]{1,0:T(1,128)} %bitcast.23, bf16[64,2048]{1,0:T(8,128)(2,1)} %bitcast.20, f32[2,128,4096]{2,1,0:T(8,128)} %refs_3_.1, ...), custom_call_target="tpu_custom_call" | custom-call | tf_op jit(solution)/shard_map/layer/pallas_call | solution.py:604
  83.0 2.3 %finish.1 = (f32[2,128,4096]{2,1,0:T(8,128)}, bf16[128,2048]{1,0:T(8,128)(2,1)}) custom-call(f32[2,128,4096]{2,1,0:T(8,128)S(1)} %get-tuple-element.8.state_ref, bf16[128,2048]{1,0:T(8,128)(2,1)S(1)} %get-tuple-element.9.resid_ref, bf16[128,256]{1,0:T(8,128)(2,1)S(1)} %get-tuple-element.10.place_ref, bf16[4,64,2048]{2,1,0:T(8,128)(2,1)S(1)} %get-tuple-element.11.returned_ref), custom_call_target="tpu_custom_call" | custom-call | tf_op jit(solution)/shard_map/finish/pallas_call | solution.py:652
